TPU v7x, 32 devices: a whole 2x2x4 slice. The times are simulated.
32 devices in a mesh: sp: 8 (over z, y), tp: 4 (over x, core).
Axes of the slice: x: 2, y: 2, z: 4, core: 2. Of those that a mesh axis runs over, the one named last changes fastest.
Arguments:
- tokens: bfloat16 [6144, 2048], P('sp', 'tp'), may hold values from -6 to 6
- norm_gain: float32 [2048], replicated, may hold values from 0.1 to 1.9
- w_query: bfloat16 [2048, 2048], P(None, 'tp'), may hold values from -4 to 4
- w_key: bfloat16 [2048, 2048], P(None, 'tp'), may hold values from -4 to 4
- w_value: bfloat16 [2048, 2048], P(None, 'tp'), may hold values from -0.125 to 0.125
- w_outer: bfloat16 [2048, 2048], P(None, 'tp'), may hold values from -0.125 to 0.125
- w_inner: bfloat16 [2048, 2048], P(None, 'tp'), may hold values from -0.125 to 0.125
- w_signal: bfloat16 [2048, 2048], P(None, 'tp'), may hold values from -0.125 to 0.125
- conv_taps: bfloat16 [3, 2048], P(None, 'tp'), may hold values from -3.5 to 3.5
- lambdas: float32 [8], P('tp'), may hold values from 0.3 to 0.8
- head_gain: float32 [256], replicated, may hold values from 0.1 to 1.9
- attend_proj: bfloat16 [2048, 2048], P('tp'), may hold values from -0.125 to 0.125
- convolve_proj: bfloat16 [2048, 2048], P('tp'), may hold values from -0.125 to 0.125
Outputs:
- mixed: bfloat16 [6144, 2048], P(('sp', 'tp'))
- row_lse: float32 [6144, 16], P('sp', 'tp')
All inputs are finite; a program needn't handle non-finite values.
Results may differ from a plain program's by a relative error of at most 0.015.
Values may be sent and summed in bfloat16 or wider, within the bound.
A program may use at most 128 MiB of HBM per device.

v0:
```python
import functools
import math

import jax
import jax.numpy as jnp
from jax import lax
from jax.experimental import pallas as pl
from jax.experimental.pallas import tpu as pltpu
from jax.sharding import PartitionSpec as P

ROPE_BASE = 500000.0
NORM_EPS = 1e-05
HEAD_KEEP = 0.8
MASKED = -1e30
LOG2E = math.log2(math.e)
MESH = pl.DeviceIdType.MESH


def partner(value, axis, stride):
    return lax.ppermute(value, axis, [(i, i ^ 1 << stride) for i in range(lax.axis_size(axis))])


def passed_along(value, axis, steps):
    count = lax.axis_size(axis)
    initial, last = (max(0, -steps), min(count, count - steps))
    return lax.ppermute(value, axis, [(source, source + steps) for source in range(initial, last)])


def rotate(values_in, positions):
    half_width = values_in.shape[-1] // 2
    inverse = ROPE_BASE ** (-jnp.arange(half_width, dtype=jnp.float32) * 2.0 / values_in.shape[-1])
    angles = positions.astype(jnp.float32)[:, None] * inverse[None, :]
    cosine = jnp.cos(angles)[:, None, :]
    sine_part = jnp.sin(angles)[:, None, :]
    first_half = values_in[..., :half_width]
    second_half = values_in[..., half_width:]
    return jnp.concatenate(
        [
            first_half * cosine - second_half * sine_part,
            second_half * cosine + first_half * sine_part,
        ],
        axis=-1,
    )


def absorb(state, queries, positions, key_block, value_block, first_key):
    running_max, weight_sum, weighted = state
    head_count = weighted.shape[0]
    block_rows = key_block.shape[0]
    scores = jnp.einsum("qgd,kgd->gqk", queries, key_block, preferred_element_type=jnp.float32)
    scores = scores * queries.shape[-1] ** (-0.5)
    key_places = first_key + jnp.arange(block_rows, dtype=jnp.int32)
    allowed = key_places[None, :] <= positions[:, None]
    scores = jnp.where(allowed[None], scores, MASKED)
    scores = scores.reshape(head_count, 2, positions.shape[0], block_rows)
    raised = jnp.maximum(running_max, jnp.max(scores, axis=3))
    factor = jnp.exp(running_max - raised)
    lifted = jnp.exp(scores - raised[..., None])
    weight_sum = factor * weight_sum + jnp.sum(lifted, axis=3)
    values_here = value_block.reshape(block_rows, head_count, -1)
    weighted = factor[..., None] * weighted + jnp.einsum(
        "hjqk,khe->hjqe",
        lifted.astype(jnp.bfloat16),
        values_here,
        preferred_element_type=jnp.float32,
    )
    return (raised, weight_sum, weighted)


def empty_state(head_count, rows, head_width):
    return (
        jnp.full((head_count, 2, rows), MASKED, jnp.float32),
        jnp.zeros((head_count, 2, rows), jnp.float32),
        jnp.zeros((head_count, 2, rows, 2 * head_width), jnp.float32),
    )


def finish(state, lambdas, head_gain):
    running_max, weight_sum, weighted = state
    head_count = weighted.shape[0]
    rows = weighted.shape[2]
    normalized = weighted / weight_sum[..., None]
    difference = normalized[:, 0] - lambdas[:, None, None] * normalized[:, 1]
    scale_back = lax.rsqrt(jnp.mean(difference * difference, axis=2, keepdims=True) + NORM_EPS)
    attended = (difference * scale_back * head_gain[None, None, :] * HEAD_KEEP).astype(jnp.bfloat16)
    attended = jnp.transpose(attended, (1, 0, 2)).reshape(rows, head_count * weighted.shape[3])
    row_lse = jnp.transpose(running_max + jnp.log(weight_sum), (2, 0, 1)).reshape(
        rows, 2 * head_count
    )
    return (attended, row_lse)


def project_kernel(scale, tok_ref, gain_ref, wq_ref, wk_ref, wv_ref, cos_ref, sin_ref, q_ref, kv_ref):
    heads, _, pair = q_ref.shape
    width = pair // 2
    widened = tok_ref[...].astype(jnp.float32)
    scaled = (widened * gain_ref[...]).astype(jnp.bfloat16)
    mean = jnp.sum(widened * widened, axis=1, keepdims=True) / widened.shape[1]
    inv_rms = lax.rsqrt(mean + NORM_EPS)
    cosine, sine = cos_ref[...], sin_ref[...]

    def rotary(x):
        return x * cosine + pltpu.roll(x, width // 2, 1) * sine

    q = jnp.dot(scaled, wq_ref[...], preferred_element_type=jnp.float32) * inv_rms
    k = jnp.dot(scaled, wk_ref[...], preferred_element_type=jnp.float32) * inv_rms
    v = jnp.dot(scaled, wv_ref[...], preferred_element_type=jnp.float32) * inv_rms
    for head in range(heads):
        for j in range(2):
            cols = slice((2 * head + j) * width, (2 * head + j + 1) * width)
            place = slice(j * width, (j + 1) * width)
            q_ref[head, :, place] = (rotary(q[:, cols]) * scale).astype(jnp.bfloat16)
            kv_ref[head, :, place] = rotary(k[:, cols]).astype(jnp.bfloat16)
        kv_ref[head, :, pair:] = v[:, head * pair : (head + 1) * pair].astype(jnp.bfloat16)


def project(tokens, norm_gain, w_query, w_key, w_value, positions, head_count, head_width):
    rows, model_width = tokens.shape
    half = head_width // 2
    inverse = ROPE_BASE ** (-jnp.arange(half, dtype=jnp.float32) * 2.0 / head_width)
    angles = positions.astype(jnp.float32)[:, None] * inverse[None, :]
    cosine, sine = jnp.cos(angles), jnp.sin(angles)
    cosine = jnp.concatenate([cosine, cosine], axis=1)
    sine = jnp.concatenate([-sine, sine], axis=1)
    pair = 2 * head_width
    block = rows // 3 if rows % 48 == 0 else rows
    whole = lambda shape: pl.BlockSpec(shape, lambda i: (0,) * len(shape))
    return pl.pallas_call(
        functools.partial(project_kernel, head_width ** (-0.5) * LOG2E),
        grid=(rows // block,),
        out_shape=(
            jax.ShapeDtypeStruct((head_count, rows, pair), jnp.bfloat16),
            jax.ShapeDtypeStruct((head_count, rows, 2 * pair), jnp.bfloat16),
        ),
        in_specs=[
            pl.BlockSpec((block, model_width), lambda i: (i, 0)),
            whole((1, model_width)),
            whole(w_query.shape),
            whole(w_key.shape),
            whole(w_value.shape),
            pl.BlockSpec((block, head_width), lambda i: (i, 0)),
            pl.BlockSpec((block, head_width), lambda i: (i, 0)),
        ],
        out_specs=(
            pl.BlockSpec((head_count, block, pair), lambda i: (0, i, 0)),
            pl.BlockSpec((head_count, block, 2 * pair), lambda i: (0, i, 0)),
        ),
        compiler_params=pltpu.CompilerParams(vmem_limit_bytes=48 * 2**20),
        cost_estimate=pl.CostEstimate(
            flops=6 * rows * model_width * w_query.shape[1],
            bytes_accessed=2 * (rows * model_width + 3 * w_query.size + 3 * rows * w_query.shape[1]),
            transcendentals=0,
        ),
        name="project_qkv",
    )(tokens, norm_gain[None, :], w_query, w_key, w_value, cosine, sine)


def attend_kernel(
    groups,
    block,
    q_pair,
    kv_pair,
    lambdas_ref,
    gain_ref,
    out_ref,
    lse_ref,
    kv_all,
    q_own,
    acc,
    top,
    total,
    local_sem,
    send_right,
    recv_sem,
    swap_send,
    swap_recv,
):
    sp = lax.axis_index("sp")
    tp = lax.axis_index("tp")
    g, y = sp // 2, sp % 2
    _, rows, pair = q_pair.shape
    width = pair // 2
    blocks = rows // block

    def at(group, place):
        return (2 * group + place, tp)

    loads = (
        pltpu.make_async_copy(kv_pair.at[y], kv_all.at[sp], local_sem.at[0]),
        pltpu.make_async_copy(q_pair.at[y], q_own.at[y], local_sem.at[1]),
    )
    for load in loads:
        load.start()
    barrier = pltpu.get_barrier_semaphore()
    pl.semaphore_signal(barrier, inc=1, device_id=at(g, 1 - y), device_id_type=MESH)

    @pl.when(g > 0)
    def _():
        pl.semaphore_signal(barrier, inc=1, device_id=at(g - 1, y), device_id_type=MESH)

    @pl.when(g < groups - 1)
    def _():
        pl.semaphore_signal(barrier, inc=1, device_id=at(g + 1, y), device_id_type=MESH)

    beside = jnp.where(g > 0, 1, 0) + jnp.where(g < groups - 1, 1, 0)
    pl.semaphore_wait(barrier, 1 + beside)

    def swap(source, target, index):
        return pltpu.make_async_remote_copy(
            src_ref=source,
            dst_ref=target,
            send_sem=swap_send.at[index],
            recv_sem=swap_recv.at[index],
            device_id=at(g, 1 - y),
            device_id_type=MESH,
        )

    swaps = (
        swap(kv_pair.at[1 - y], kv_all.at[sp], 0),
        swap(q_pair.at[1 - y], q_own.at[y], 1),
    )
    for one_swap in swaps:
        one_swap.start()
    loads[0].wait()

    def right(chunk):
        return pltpu.make_async_remote_copy(
            src_ref=kv_all.at[chunk],
            dst_ref=kv_all.at[chunk],
            send_sem=send_right.at[chunk],
            recv_sem=recv_sem.at[chunk],
            device_id=at(jnp.minimum(g + 1, groups - 1), y),
            device_id_type=MESH,
        )

    @pl.when(g < groups - 1)
    def _():
        right(sp).start()

    acc[...] = jnp.zeros_like(acc)
    total[...] = jnp.zeros_like(total)
    top[...] = jnp.full_like(top, MASKED)

    def update(r, j, start, scores, values):
        here = pl.ds(start, block)
        old = top[r, j, here, :]
        new = jnp.maximum(old, jnp.max(scores, axis=1, keepdims=True))
        shrink = jnp.exp2(old - new)
        lifted = jnp.exp2(scores - new[:, :1])
        top[r, j, here, :] = new
        total[r, j, here, :] = shrink * total[r, j, here, :] + jnp.sum(lifted, axis=1, keepdims=True)
        acc[r, j, here, :] = shrink[:, :1] * acc[r, j, here, :] + jnp.dot(
            lifted.astype(jnp.bfloat16), values, preferred_element_type=jnp.float32
        )

    def scores_of(r, j, start, chunk, length):
        cols = slice(j * width, (j + 1) * width)
        queries = q_own[r, pl.ds(start, block), cols]
        keys = kv_all[chunk, :length, cols]
        return lax.dot_general(
            queries, keys, (((1,), (1,)), ((), ())), preferred_element_type=jnp.float32
        )

    def process(r, chunk):
        q_chunk = 2 * g + r

        @pl.when(chunk < q_chunk)
        def _():
            def one(b, carry):
                start = pl.multiple_of(b * block, block)
                for j in range(2):
                    update(r, j, start, scores_of(r, j, start, chunk, rows), kv_all[chunk, :, pair:])
                return carry

            lax.fori_loop(0, blocks, one, 0)

        @pl.when(chunk == q_chunk)
        def _():
            for b in range(blocks):
                length = (b + 1) * block
                query_at = b * block + lax.broadcasted_iota(jnp.int32, (block, length), 0)
                key_at = lax.broadcasted_iota(jnp.int32, (block, length), 1)
                for j in range(2):
                    scores = scores_of(r, j, b * block, chunk, length)
                    scores = jnp.where(key_at <= query_at, scores, MASKED)
                    update(r, j, b * block, scores, kv_all[chunk, :length, pair:])

    loads[1].wait()
    swaps[0].wait()

    @pl.when(g < groups - 1)
    def _():
        right(2 * g + 1 - y).start()

    swaps[1].wait()

    def visit(i, carry):
        step, half = i // 2, i % 2
        group = g - step
        chunk = 2 * group + jnp.where(half == 0, y, 1 - y)

        @pl.when(step > 0)
        def _():
            right(chunk).wait_recv()

            @pl.when(g < groups - 1)
            def _():
                right(chunk).start()

        def each(r, inner):
            process(r, chunk)
            return inner

        lax.fori_loop(0, 2, each, 0)
        return carry

    lax.fori_loop(0, 2 * g + 2, visit, 0)

    lam = lambdas_ref[y]
    gain = gain_ref[...] * HEAD_KEEP

    def close(i, carry):
        r, start = i // blocks, pl.multiple_of((i % blocks) * block, block)
        here = pl.ds(start, block)
        sums = [total[r, j, here, :] for j in range(2)]
        parts = [acc[r, j, here, :] / sums[j][:, :1] for j in range(2)]
        difference = parts[0] - lam * parts[1]
        mean = jnp.mean(difference * difference, axis=1, keepdims=True)
        out_ref[r, here, :] = (difference * lax.rsqrt(mean + NORM_EPS) * gain).astype(jnp.bfloat16)
        lses = [top[r, j, here, :] * (1.0 / LOG2E) + jnp.log(sums[j]) for j in range(2)]
        lane = lax.broadcasted_iota(jnp.int32, lses[0].shape, 1)
        lse_ref[r, here, :] = jnp.where(lane == 0, lses[0], lses[1])
        return carry

    lax.fori_loop(0, 2 * blocks, close, 0)

    def drain(chunk, carry):
        right(chunk).wait_send()
        return carry

    @pl.when(g < groups - 1)
    def _():
        lax.fori_loop(0, 2 * g + 2, drain, 0)


def attend(groups, q_pair, kv_pair, lambdas, head_gain):
    _, rows, pair = q_pair.shape
    block = rows // 3 if rows % 48 == 0 else rows
    vmem = pl.BlockSpec(memory_space=pltpu.VMEM)
    anywhere = pl.BlockSpec(memory_space=pl.ANY)
    chunks = 2 * groups
    lanes = 128
    return pl.pallas_call(
        functools.partial(attend_kernel, groups, block),
        out_shape=(
            jax.ShapeDtypeStruct((2, rows, pair), jnp.bfloat16),
            jax.ShapeDtypeStruct((2, rows, lanes), jnp.float32),
        ),
        in_specs=[anywhere] * 2 + [pl.BlockSpec(memory_space=pltpu.SMEM), vmem],
        out_specs=(vmem, vmem),
        scratch_shapes=[
            pltpu.VMEM((chunks, rows, 2 * pair), jnp.bfloat16),
            pltpu.VMEM((2, rows, pair), jnp.bfloat16),
            pltpu.VMEM((2, 2, rows, pair), jnp.float32),
            pltpu.VMEM((2, 2, rows, lanes), jnp.float32),
            pltpu.VMEM((2, 2, rows, lanes), jnp.float32),
            pltpu.SemaphoreType.DMA((2,)),
            pltpu.SemaphoreType.DMA((chunks,)),
            pltpu.SemaphoreType.DMA((chunks,)),
            pltpu.SemaphoreType.DMA((2,)),
            pltpu.SemaphoreType.DMA((2,)),
        ],
        compiler_params=pltpu.CompilerParams(
            collective_id=0, has_side_effects=True, vmem_limit_bytes=56 * 2**20
        ),
        cost_estimate=pl.CostEstimate(
            flops=8 * chunks * rows * rows * 3 * pair // 4,
            bytes_accessed=8 * rows * pair,
            transcendentals=0,
        ),
        name="attend_line",
    )(q_pair, kv_pair, lambdas, head_gain[None, :])


def attention_by_head(tokens, norm_gain, w_query, w_key, w_value, lambdas, head_gain, positions):
    head_count = lambdas.shape[0]
    head_width = w_query.shape[1] // (2 * head_count)
    count = lax.axis_size("sp")
    groups = count // 2
    y = lax.axis_index("sp") % 2
    queries, key_values = project(
        tokens, norm_gain, w_query, w_key, w_value, positions, head_count, head_width
    )
    result, lse = attend(groups, queries, key_values, lambdas, head_gain)
    lse = lse[:, :, :2]
    at_first = y == 0
    crossed = partner(jnp.where(at_first, result[1], result[0]), "sp", 0)
    crossed_lse = partner(jnp.where(at_first, lse[1], lse[0]), "sp", 0)
    first = jnp.where(at_first, result[0], crossed)
    last = jnp.where(at_first, crossed, result[1])
    first_lse = jnp.where(at_first, lse[0], crossed_lse)
    last_lse = jnp.where(at_first, crossed_lse, lse[1])
    return (
        jnp.concatenate([first, last], axis=1),
        jnp.concatenate([first_lse, last_lse], axis=1),
    )


def make_fold(groups, row_count, carry, pieces):
    key_piece, value_piece = pieces
    block_rows = min(key_piece.shape[0], row_count)
    shard_count = key_piece.shape[0] // block_rows

    def one_shard(inner_states, shard_index):
        first_key = shard_index * block_rows
        key_block = lax.dynamic_slice_in_dim(key_piece, shard_index * block_rows, block_rows, 0)
        value_block = lax.dynamic_slice_in_dim(value_piece, shard_index * block_rows, block_rows, 0)
        updated_states = []
        for given_state, group in zip(inner_states, groups):
            group_queries, group_places, group_last = group

            def take_block(given):
                return absorb(given, group_queries, group_places, key_block, value_block, first_key)

            def leave_block(given):
                return given

            updated_states.append(
                lax.cond(first_key < group_last, take_block, leave_block, given_state)
            )
        return (tuple(updated_states), None)

    carry, _ = lax.scan(one_shard, carry, jnp.arange(shard_count, dtype=jnp.int32))
    return carry


def attention_by_rows(query_sums, key_sums, value_sums, lambdas, head_gain, positions):
    row_count = query_sums.shape[0]
    head_count = lambdas.shape[0]
    head_width = query_sums.shape[1] // (2 * head_count)
    offset = lax.axis_index("sp") * row_count
    split = (row_count, 2 * head_count, head_width)
    queries = rotate(query_sums.reshape(split), positions).astype(jnp.bfloat16)
    key_rows = rotate(key_sums.reshape(split), positions).astype(jnp.bfloat16)
    value_rows = value_sums.astype(jnp.bfloat16)
    half_rows = row_count // 2
    bit_count = lax.axis_size("sp").bit_length() - 1
    handed = queries[half_rows:]
    for bit_index in range(bit_count):
        handed = partner(handed, "sp", bit_index)
    mirror = lax.axis_size("sp") - 1 - lax.axis_index("sp")
    mirror_start = mirror * row_count + half_rows
    mirror_places = mirror_start + jnp.arange(half_rows, dtype=jnp.int32)
    groups = (
        (queries[:half_rows], positions[:half_rows], offset + half_rows),
        (handed, mirror_places, mirror_start + half_rows),
    )
    initial = (
        empty_state(head_count, half_rows, head_width),
        empty_state(head_count, half_rows, head_width),
    )
    states = make_fold(
        groups,
        row_count,
        initial,
        (
            lax.all_gather(key_rows, "sp", axis=0, tiled=True),
            lax.all_gather(value_rows, "sp", axis=0, tiled=True),
        ),
    )
    own_attended, own_lse = finish(states[0], lambdas, head_gain)
    answer = finish(states[1], lambdas, head_gain)
    for bit_index in range(bit_count):
        answer = (
            partner(answer[0], "sp", bit_index),
            partner(answer[1].astype(jnp.bfloat16), "sp", bit_index).astype(jnp.float32),
        )
    attended = jnp.concatenate([own_attended, answer[0]], axis=0)
    row_lse = jnp.concatenate([own_lse, answer[1]], axis=0)
    return (attended, row_lse)


def per_device(
    tokens,
    norm_gain,
    w_query,
    w_key,
    w_value,
    w_outer,
    w_inner,
    w_signal,
    conv_taps,
    lambdas,
    head_gain,
    attend_proj,
    convolve_proj,
):
    row_count = tokens.shape[0]
    model_width = norm_gain.shape[0]
    head_count = lambdas.shape[0]
    head_width = w_query.shape[1] // (2 * head_count)
    count = lax.axis_size("sp")
    gathered = lax.all_gather(tokens, "tp", axis=1, tiled=True)
    widened = gathered.astype(jnp.float32)
    scaled = (widened * norm_gain[None, :]).astype(jnp.bfloat16)
    squares = jnp.sum(widened * widened, axis=1)
    inv_rms = lax.rsqrt(squares / model_width + NORM_EPS)[:, None]
    offset = lax.axis_index("sp") * row_count
    positions = offset + jnp.arange(row_count, dtype=jnp.int32)

    def product_of(weight):
        return inv_rms * jnp.dot(scaled, weight, preferred_element_type=jnp.float32)

    if head_count == 2 and head_width == 128 and count % 2 == 0:
        attended, row_lse = attention_by_head(
            gathered, norm_gain, w_query, w_key, w_value, lambdas, head_gain, positions
        )
    else:
        attended, row_lse = attention_by_rows(
            product_of(w_query),
            product_of(w_key),
            product_of(w_value),
            lambdas,
            head_gain,
            positions,
        )
    outer_gate = product_of(w_outer)
    product = product_of(w_inner) * product_of(w_signal)
    border = passed_along(product[row_count - 2 :], "sp", 1)
    padded = jnp.concatenate([border, product], axis=0)
    tap_values = conv_taps.astype(jnp.float32)
    smoothed = (
        tap_values[0] * padded[:-2] + tap_values[1] * padded[1:-1] + tap_values[2] * padded[2:]
    )
    convolved = (outer_gate * smoothed).astype(jnp.bfloat16)
    mixed = lax.psum_scatter(
        (
            jnp.dot(attended, attend_proj, preferred_element_type=jnp.float32)
            + jnp.dot(convolved, convolve_proj, preferred_element_type=jnp.float32)
        ).astype(jnp.bfloat16),
        "tp",
        scatter_dimension=0,
        tiled=True,
    )
    return (mixed, row_lse)


def solution(mesh):
    return jax.shard_map(
        per_device,
        mesh=mesh,
        in_specs=(
            P("sp", "tp"),
            P(),
            P(None, "tp"),
            P(None, "tp"),
            P(None, "tp"),
            P(None, "tp"),
            P(None, "tp"),
            P(None, "tp"),
            P(None, "tp"),
            P("tp"),
            P(),
            P("tp", None),
            P("tp", None),
        ),
        out_specs=(P(("sp", "tp"), None), P("sp", "tp")),
        check_vma=False,
    )
```

profile of v0, /device:TPU:6, one launch (start us, length us, event | category | flops | bytes accessed | tf_op | source)
XLA Modules:
  0.0 240.2 jit_solution(8771024620407991104)
XLA Ops:
  7.2 0.0 copy-start
  7.2 0.0 copy-start.8
  7.2 0.0 all-gather.2.cloned.1.call-start
  7.2 0.7 all-gather.2.cloned.1.call-update
  7.9 0.0 reduce-scatter.2.cloned.1.call-start
  8.0 1.4 fusion.29
  9.5 0.0 copy-start.2
  9.5 0.3 pad_maximum_fusion.1
  9.8 0.0 copy-done.8
  9.8 28.6 %all-gather.2.cloned.1.call-done.tok_ref = bf16[768,2048]{1,0:T(8,128)(2,1)} async-done(((bf16[768,512]{1,0:T(8,128)(2,1)}), bf16[768,2048]{1,0:T(8,128)(2,1)}) %all-gather.2.cloned.1.call-update) | async-done | bytes 3145744 | tf_op jit(solution)/shard_map/all_gather | solution.py:503
  38.4 0.0 copy-start.5
  38.4 2.7 %fusion = f32[768]{0:T(1024)S(1)} fusion(bf16[768,2048]{1,0:T(8,128)(2,1)} %all-gather.2.cloned.1.call-done.tok_ref), kind=kLoop, calls=%fused_computation.2 | loop fusion | flops 4717824 | bytes 3148800 | tf_op jit(solution)/shard_map/reduce_sum | solution.py:506
  41.1 0.0 copy-done.2
  41.1 0.1 copy-done.5
  41.2 0.0 copy-start.10
  41.2 3.5 %fusion.2 = f32[768,512]{1,0:T(8,128)S(1)} fusion(bf16[2048,512]{1,0:T(8,128)(2,1)} %param.20, bf16[768,2048]{1,0:T(8,128)(2,1)S(1)} %copy-done.5, f32[2048]{0:T(1024)S(1)} %copy-done.2), kind=kOutput, calls=%fused_computation.5 | convolution fusion | flops 1615331328 | bytes 6823936 | tf_op jit(solution)/shard_map/dot_general | solution.py:512
  44.7 0.0 copy-done.10
  44.8 0.0 copy-start.1
  44.8 1.8 multiply_multiply_fusion
  46.6 0.0 copy-start.9
  46.6 3.4 %collective-permute-start.1 = (f32[2,512]{1,0:T(2,128)S(1)}, f32[2,512]{1,0:T(2,128)S(1)}, u32[]{:S(2)}, u32[]{:S(2)}) collective-permute-start(f32[2,512]{1,0:T(2,128)S(1)} %slice.48), channel_id=1, source_target_pairs={{0,4},{4,8},{8,12},{12,16},{16,20},{20,24},{24,28},{1,5},{5,9},{9,... | collective-permute-start | bytes 12296 | tf_op jit(solution)/shard_map/ppermute | solution.py:26
  50.0 0.0 copy-done.9
  50.0 0.0 copy-done.1
  50.0 8.5 %project_qkv.1 = (bf16[2,768,256]{2,1,0:T(8,128)(2,1)S(1)}, bf16[2,768,512]{2,1,0:T(8,128)(2,1)S(1)}) custom-call(bf16[768,2048]{1,0:T(8,128)(2,1)} %all-gather.2.cloned.1.call-done.tok_ref, f32[1,2048]{1,0:T(1,128)S(1)} %bitcast.22, bf16[2048,512]{1,0:T(8,128)(2,1)S(1)} %copy-done.1, bf16[2048,512]{1,0:T(8,128)(2,1)} %wk_ref.1, bf16[2048,512]{1,0:T(8,128)(2,1)} %wv_ref.1, ...), custom_call_target="tpu_custom_call" | custom-call | flops 4831838208 | bytes 11796480 | tf_op jit(solution)/shard_map/project_qkv/pallas_call | solution.py:128
  58.5 0.0 copy-start.3
  58.5 1.2 copy-done.3
  59.6 0.0 copy-start.4
  59.6 0.9 copy-done.4
  60.5 40.4 %attend_line.1 = (bf16[2,768,256]{2,1,0:T(8,128)(2,1)}, f32[2,768,128]{2,1,0:T(8,128)}) custom-call(bf16[2,768,256]{2,1,0:T(8,128)(2,1)} %copy-done.4, bf16[2,768,512]{2,1,0:T(8,128)(2,1)} %copy-done.3, f32[2]{0:T(128)} %lambdas_ref.1, f32[1,256]{1,0:T(1,128)} %bitcast.26), custom_call_target="tpu_custom_call" | custom-call | flops 7247757312 | bytes 1572864 | tf_op jit(solution)/shard_map/attend_line/pallas_call | solution.py:353
  101.0 1.9 bitcast_select_fusion.4
  102.9 1.5 collective-permute-start
  104.4 0.0 collective-permute-done.1
  104.4 0.0 copy-done
  104.4 0.0 copy-start.7
  104.4 10.4 %fusion.20 = f32[768,2048]{1,0:T(8,128)} fusion(bf16[512,2048]{1,0:T(8,128)(2,1)S(1)} %copy-done, f32[2,512]{1,0:T(2,128)S(1)} %collective-permute-done.1, f32[768,512]{1,0:T(8,128)} %copy-done.9, bf16[2048,512]{1,0:T(8,128)(2,1)} %param.18, bf16[768,2048]{1,0:T(8,128)(2,1)} %all-gather.2.cloned.1.call-done.tok_ref, f32[2048]{0:T(1024)S(1)} %copy-done.2, ...), kind=kOutput, calls=%fused_computation.19 | convolution fusion | flops 3229876224 | bytes 15225856 | tf_op jit(solution)/shard_map/dot_general | solution.py:539
  114.8 0.0 collective-permute-done
  114.8 0.0 copy-done.7
  114.8 0.1 bitcast_select_fusion.5
  114.9 7.0 %add_convert_fusion = bf16[768,2048]{1,0:T(8,128)(2,1)} fusion(f32[768,2048]{1,0:T(8,128)} %fusion.20, bf16[512,2048]{1,0:T(8,128)(2,1)} %param.24, bf16[768,256]{1,0:T(8,128)(2,1)S(1)} %get-tuple-element.15, bf16[768,256]{1,0:T(8,128)(2,1)S(1)} %get-tuple-element.14), kind=kOutput, calls=%fused_computation.4 | convolution fusion | flops 1615331328 | bytes 12320768 | tf_op jit(solution)/shard_map/dot_general | solution.py:538
  121.8 0.0 copy-start.6
  121.8 0.0 reduce-scatter.2.cloned.1.call-update
  121.9 1.1 copy-done.6
  123.0 0.6 collective-permute-start.2
  123.6 9.3 %collective-permute-done.2 = f32[768,2]{1,0:T(8,128)S(1)} collective-permute-done((f32[768,2]{1,0:T(8,128)S(1)}, f32[768,2]{1,0:T(8,128)S(1)}, u32[]{:S(2)}, u32[]{:S(2)}) %collective-permute-start.2) | collective-permute-done | bytes 6176 | tf_op jit(solution)/shard_map/ppermute | solution.py:20
  132.9 0.8 bitcast_select_fusion.2
  133.7 1.1 copy.16
  134.9 0.2 copy.17
  135.0 0.6 pad_maximum_fusion.3
  135.6 97.7 %reduce-scatter.2.cloned.1.call-done = bf16[192,2048]{1,0:T(8,128)(2,1)} async-done(((bf16[768,2048]{1,0:T(8,128)(2,1)}), bf16[192,2048]{1,0:T(8,128)(2,1)}) %reduce-scatter.2.cloned.1.call-update) | async-done | bytes 786448 | tf_op jit(solution)/shard_map/reduce_scatter | solution.py:536
  (6 shorter events, 0.1 us)
Async XLA Ops:
  7.2 97.2 %copy-start = (bf16[512,2048]{1,0:T(8,128)(2,1)S(1)}, bf16[512,2048]{1,0:T(8,128)(2,1)}, u32[]{:S(2)}) copy-start(bf16[512,2048]{1,0:T(8,128)(2,1)} %param.25) | copy-start | bytes 6291460
  7.2 2.6 %copy-start.8 = (bf16[3,512]{1,0:T(4,128)(2,1)S(1)}, bf16[3,512]{1,0:T(4,128)(2,1)}, u32[]{:S(2)}) copy-start(bf16[3,512]{1,0:T(4,128)(2,1)} %param.21) | copy-start | bytes 9220
  7.2 31.2 %all-gather.2.cloned.1.call-start = ((), (), s32[]{:S(2)}) async-start(), calls=%async_computation.1 | async-start | bytes 3932160 | tf_op jit(solution)/shard_map/all_gather | solution.py:503
  7.9 225.4 %reduce-scatter.2.cloned.1.call-start = ((), (), s32[]{:S(2)}) async-start(), calls=%async_computation.2 | async-start | bytes 3932160 | tf_op jit(solution)/shard_map/reduce_scatter | solution.py:536
  9.5 31.6 %copy-start.2 = (f32[2048]{0:T(1024)S(1)}, f32[2048]{0:T(1024)}, u32[]{:S(2)}) copy-start(f32[2048]{0:T(1024)} %param.14) | copy-start | bytes 24580
  38.4 2.8 %copy-start.5 = (bf16[768,2048]{1,0:T(8,128)(2,1)S(1)}, bf16[768,2048]{1,0:T(8,128)(2,1)}, u32[]{:S(2)}) copy-start(bf16[768,2048]{1,0:T(8,128)(2,1)} %all-gather.2.cloned.1.call-done.tok_ref) | copy-start | bytes 9437188
  41.2 3.5 %copy-start.10 = (bf16[2048,512]{1,0:T(8,128)(2,1)S(1)}, bf16[2048,512]{1,0:T(8,128)(2,1)}, u32[]{:S(2)}) copy-start(bf16[2048,512]{1,0:T(8,128)(2,1)} %param.19) | copy-start | bytes 6291460
  44.8 5.3 %copy-start.1 = (bf16[2048,512]{1,0:T(8,128)(2,1)S(1)}, bf16[2048,512]{1,0:T(8,128)(2,1)}, u32[]{:S(2)}) copy-start(bf16[2048,512]{1,0:T(8,128)(2,1)} %wq_ref.1) | copy-start | bytes 6291460
  46.6 3.4 %copy-start.9 = (f32[768,512]{1,0:T(8,128)}, f32[768,512]{1,0:T(8,128)S(1)}, u32[]{:S(2)}) copy-start(f32[768,512]{1,0:T(8,128)S(1)} %multiply_multiply_fusion) | copy-start | bytes 4718596
  46.6 57.8 %collective-permute-start.1 = (f32[2,512]{1,0:T(2,128)S(1)}, f32[2,512]{1,0:T(2,128)S(1)}, u32[]{:S(2)}, u32[]{:S(2)}) collective-permute-start(f32[2,512]{1,0:T(2,128)S(1)} %slice.48), channel_id=1, source_target_pairs={{0,4},{4,8},{8,12},{12,16},{16,20},{20,24},{24,28},{1,5},{5,9},{9,... | collective-permute-start | bytes 12296 | tf_op jit(solution)/shard_map/ppermute | solution.py:26
  58.5 1.2 copy-start.3
  59.6 0.9 copy-start.4
  102.9 11.9 %collective-permute-start = (bf16[768,256]{1,0:T(8,128)(2,1)}, bf16[768,256]{1,0:T(8,128)(2,1)S(1)}, u32[]{:S(2)}, u32[]{:S(2)}) collective-permute-start(bf16[768,256]{1,0:T(8,128)(2,1)} %bitcast_select_fusion.4), channel_id=1, source_target_pairs={{0,4},{4,0},{8,12},{12,8},{16,20},{20,16},{24,28},{28,24},{1,5},{5... | collective-permute-start | bytes 1179656 | tf_op jit(solution)/shard_map/ppermute | solution.py:20
  104.4 10.4 %copy-start.7 = (bf16[2,768,256]{2,1,0:T(8,128)(2,1)S(1)}, bf16[2,768,256]{2,1,0:T(8,128)(2,1)}, u32[]{:S(2)}) copy-start(bf16[2,768,256]{2,1,0:T(8,128)(2,1)} %get-tuple-element.8) | copy-start | bytes 2359300
  121.8 1.1 copy-start.6
  123.0 9.9 %collective-permute-start.2 = (f32[768,2]{1,0:T(8,128)S(1)}, f32[768,2]{1,0:T(8,128)S(1)}, u32[]{:S(2)}, u32[]{:S(2)}) collective-permute-start(f32[768,2]{1,0:T(8,128)S(1)} %bitcast_select_fusion.1), channel_id=1, source_target_pairs={{0,4},{4,0},{8,12},{12,8},{16,20},{20,16},{24,28},{28,24},{1,5},{5... | collective-permute-start | bytes 18440 | tf_op jit(solution)/shard_map/ppermute | solution.py:20
Sparse Core Ops, SparseCore 0:
  9.6 28.7 all-gather.1
  122.0 111.3 reduce-scatter.1
where the time goes:
time: 243 us; the launch traced here: 240 us
  waiting for transfers between devices  136 us (56%)
  Pallas kernels  48.9 us (20%)
  matrix products  22.7 us (9%)
  between operations  14.2 us (6%)
  other arithmetic  7.91 us (3%)
  starting transfers between devices  5.55 us (2%)
  local copies, waits for them, and re-layouts  4.59 us (2%)
    reduce_scatter x1, waiting for transfers between devices, per_device(): lax.psum_scatter((jnp.dot(attended, attend_proj, preferred_element_type=j...  97.7 us
    pallas_call x1, Pallas kernels, attend(): pl.pallas_call(functools.partial(attend_kernel, groups, block), out_shape...  40.4 us
    all_gather x1, waiting for transfers between devices, per_device(): gathered = lax.all_gather(tokens, 'tp', axis=1, tiled=True)  28.6 us
    dot_general x1, matrix products, per_device(): jnp.dot(convolved, convolve_proj, preferred_element_type=jnp.float32)  10.4 us
    ppermute x2, waiting for transfers between devices, partner(): lax.ppermute(value, axis, [(i, i ^ 1 << stride) for i in range(lax.axis_s...  9.3 us
    pallas_call x1, Pallas kernels, project(): pl.pallas_call(functools.partial(project_kernel, head_width ** (-0.5) * L...  8.45 us
    dot_general x1, matrix products, per_device(): jnp.dot(attended, attend_proj, preferred_element_type=jnp.float32)  6.98 us
    dot_general x2, matrix products, product_of(): return inv_rms * jnp.dot(scaled, weight, preferred_element_type=jnp.float32)  5.34 us
  transfers between devices with their start and end apart: 5, of which 3 were waited for; matrix products, arithmetic and copies ran while one was open for 7% of the time, Pallas kernels for 20%

commit v1 on v0

--- a/solution.py
+++ b/solution.py
@@ -3,6 +3,7 @@
 
 import jax
 import jax.numpy as jnp
+import numpy as np
 from jax import lax
 from jax.experimental import pallas as pl
 from jax.experimental.pallas import tpu as pltpu
@@ -14,6 +15,7 @@
 MASKED = -1e30
 LOG2E = math.log2(math.e)
 MESH = pl.DeviceIdType.MESH
+PIECES = 4
 
 
 def partner(value, axis, stride):
@@ -406,6 +408,682 @@
     )
 
 
+def table_of(rows, chunks, head_width):
+    half = head_width // 2
+    inverse = ROPE_BASE ** (-np.arange(half, dtype=np.float64) * 2.0 / head_width)
+    def both(places):
+        angles = places[:, None] * inverse[None, :]
+        angles = np.concatenate([angles, angles], axis=1)
+        return np.cos(angles).astype(np.float32), np.sin(angles).astype(np.float32)
+    near = both(np.arange(rows, dtype=np.float64))
+    far = both(np.arange(chunks, dtype=np.float64) * rows)
+    return np.stack(near), np.stack(far, axis=1)
+
+
+def layer_kernel(
+    tokens, w_query, w_key, w_value, w_outer, w_inner, w_signal, near_in, wa_in, wc_in,
+    gain_ref, far_ref, taps_ref, lam_ref, head_gain_ref,
+    out_ref, lse_ref,
+    tok, wqkv, wconv, wo, near, kv, q_all, q_stage, prod, gate, cv, cv_stage, att, att_stage,
+    lse_in, lse_stage, lam_in, rs_in, rs_stage, rs_keep, acc, top, total,
+    local_sem, tok_send, tok_recv, kv_to_p, kv_to_y, kv_to_z, kv_recv, q_send, q_recv,
+    cv_send, cv_recv, edge_sem, att_send, att_recv, lse_send, lse_recv, wo_send, wo_recv,
+    lam_sem, rs_send, rs_recv,
+):
+    s, t = lax.axis_index("sp"), lax.axis_index("tp")
+    x, c = t // 2, t % 2
+    y, zl, zh = s % 2, (s // 2) % 2, s // 4
+    last = lax.axis_size("sp") - 1
+    s1, s2, s4 = s + 1 - 2 * y, s + 2 - 4 * zl, s + 4 - 8 * zh
+    s6 = s4 + 2 - 4 * zl
+    t1, t2 = t + 1 - 2 * c, t + 2 - 4 * x
+    owner = c == zl
+    other = c != zl
+    rows, width = tok.shape[1], tok.shape[2]
+    block = tokens.shape[1]
+    pieces = PIECES
+    piece = rows // pieces
+    pair = wqkv.shape[1] // 3
+    hw = pair // 2
+    halves = 2 * piece
+    bf16, f32 = jnp.bfloat16, jnp.float32
+
+    def remote(src, dst, ss, rs, dev):
+        return pltpu.make_async_remote_copy(
+            src_ref=src, dst_ref=dst, send_sem=ss, recv_sem=rs, device_id=dev, device_id_type=MESH
+        )
+
+    def span(p):
+        return pl.ds(pl.multiple_of(p * piece, 16), piece)
+
+    def cols(b):
+        return pl.ds(pl.multiple_of(b * block, 128), block)
+
+    own_cols = pl.ds(pl.multiple_of(zh * pair, 128), pair)
+    loads = [
+        pltpu.make_async_copy(tokens, tok.at[0, :, cols(t)], local_sem.at[0]),
+        pltpu.make_async_copy(w_query.at[:, own_cols], wqkv.at[:, 0:pair], local_sem.at[1]),
+        pltpu.make_async_copy(w_key.at[:, own_cols], wqkv.at[:, pair : 2 * pair], local_sem.at[2]),
+        pltpu.make_async_copy(w_value.at[:, own_cols], wqkv.at[:, 2 * pair :], local_sem.at[3]),
+        pltpu.make_async_copy(near_in, near, local_sem.at[4]),
+        pltpu.make_async_copy(w_inner, wconv.at[0], local_sem.at[5]),
+        pltpu.make_async_copy(w_signal, wconv.at[1], local_sem.at[6]),
+        pltpu.make_async_copy(w_outer, wconv.at[2], local_sem.at[7]),
+        pltpu.make_async_copy(wa_in, wo.at[c], local_sem.at[8]),
+        pltpu.make_async_copy(wc_in, wo.at[2 + c], local_sem.at[9]),
+    ]
+    for load in loads:
+        load.start()
+
+    barrier = pltpu.get_barrier_semaphore()
+    peers = [(s1, t), (s2, t), (s4, t), (s6, t), (s, t1), (s, t2), (s2, t1), (s4, t1), (s6, t1)]
+    for peer in peers:
+        pl.semaphore_signal(barrier, inc=1, device_id=peer, device_id_type=MESH)
+    up_ok, down_ok = s < last, s > 0
+    up, down = jnp.minimum(s + 1, last), jnp.maximum(s - 1, 0)
+
+    @pl.when((y == 1) & up_ok)
+    def _():
+        pl.semaphore_signal(barrier, inc=1, device_id=(up, t), device_id_type=MESH)
+
+    @pl.when((y == 0) & down_ok)
+    def _():
+        pl.semaphore_signal(barrier, inc=1, device_id=(down, t), device_id_type=MESH)
+
+    across = jnp.where(y == 1, jnp.where(up_ok, 1, 0), jnp.where(down_ok, 1, 0))
+    pl.semaphore_wait(barrier, len(peers) + across)
+
+    def tok_at(k, p, b):
+        return tok.at[k, span(p), cols(b)]
+
+    def own_to_p(p):
+        return remote(tokens.at[span(p)], tok_at(0, p, t), tok_send.at[0, p], tok_recv.at[0, 1, p], (s, t1))
+
+    def own_to_x(p):
+        return remote(tokens.at[span(p)], tok_at(0, p, t), tok_send.at[1, p], tok_recv.at[0, 2, p], (s, t2))
+
+    def own_to_f(p):
+        return remote(tokens.at[span(p)], tok_at(1, p, t), tok_send.at[2, p], tok_recv.at[1, 0, p], (s4, t))
+
+    def mate_to_f(p):
+        return remote(tok_at(0, p, t1), tok_at(1, p, t1), tok_send.at[3, p], tok_recv.at[1, 1, p], (s4, t))
+
+    def cross_to_p(k, p):
+        return remote(
+            tok_at(k, p, t2), tok_at(k, p, t2), tok_send.at[4 + 4 * k, p], tok_recv.at[k, 3, p], (s, t1)
+        )
+
+    def far_to_p(p):
+        return remote(tok_at(1, p, t), tok_at(1, p, t), tok_send.at[5, p], tok_recv.at[1, 1, p], (s, t1))
+
+    def mate_back(p):
+        return remote(tok_at(1, p, t1), tok_at(1, p, t1), tok_send.at[6, p], tok_recv.at[1, 0, p], (s, t1))
+
+    def far_to_x(p):
+        return remote(tok_at(1, p, t), tok_at(1, p, t), tok_send.at[7, p], tok_recv.at[1, 2, p], (s, t2))
+
+    def tok_got(k, index, p):
+        block_of = (t, t1, t2, t1 + t2 - t)[index]
+        here = tok_at(k, p, block_of)
+        remote(here, here, tok_send.at[0, p], tok_recv.at[k, index, p], (s, t1)).wait_recv()
+
+    def each(n, body, start=0):
+        def one(i, carry):
+            body(i)
+            return carry
+
+        lax.fori_loop(start, n, one, 0)
+
+    def first_sends(p):
+        own_to_x(p).start()
+        own_to_p(p).start()
+
+    each(pieces, first_sends)
+    lam_copy = remote(lam_ref, lam_in, lam_sem.at[0], lam_sem.at[1], (s, t1))
+    lam_copy.start()
+
+    def second_sends(p):
+        tok_got(0, 1, p)
+
+        @pl.when(owner)
+        def _():
+            own_to_f(p).start()
+            mate_to_f(p).start()
+
+    each(pieces, second_sends)
+    wo_copies = (
+        remote(wa_in, wo.at[c], wo_send.at[0], wo_recv.at[0], (s, t1)),
+        remote(wc_in, wo.at[2 + c], wo_send.at[1], wo_recv.at[1], (s, t1)),
+    )
+    for one_copy in wo_copies:
+        one_copy.start()
+
+    acc[...] = jnp.zeros_like(acc)
+    total[...] = jnp.zeros_like(total)
+    top[...] = jnp.full_like(top, MASKED)
+    for load in loads:
+        load.wait()
+
+    def made(k):
+        return jnp.where(owner, 4 * k, 8 + k)
+
+    def kv_at(slot, p):
+        return kv.at[slot, span(p)]
+
+    def kv_p(slot, p):
+        return remote(kv_at(slot, p), kv_at(slot, p), kv_to_p.at[slot, p], kv_recv.at[slot, p], (s, t1))
+
+    def kv_y(slot, p):
+        return remote(
+            kv_at(slot, p), kv_at(slot + 1, p), kv_to_y.at[slot // 2, p], kv_recv.at[slot + 1, p], (s1, t)
+        )
+
+    def kv_z(k, p):
+        return remote(
+            kv_at(8 + k, p), kv_at(4 * k + 2, p), kv_to_z.at[k, p], kv_recv.at[4 * k + 2, p], (s2, t)
+        )
+
+    def q_rows(p):
+        return pl.ds(pl.multiple_of((p // 2) * piece, 16), piece)
+
+    def q_home(k, p):
+        return remote(
+            q_stage.at[k, span(p)], q_all.at[2 * k, q_rows(p)], q_send.at[k, p],
+            q_recv.at[2 * k, p // 2], (s, t1),
+        )
+
+    def q_away(k, p):
+        return remote(
+            q_stage.at[k, span(p)], q_all.at[2 * k + 1, q_rows(p)], q_send.at[k, p],
+            q_recv.at[2 * k + 1, p // 2], (s2, 2 * x + p % 2),
+        )
+
+    def ship(k, p):
+        @pl.when(owner)
+        def _():
+            kv_y(4 * k, p).start()
+            kv_p(4 * k, p).start()
+
+            @pl.when(p % 2 != c)
+            def _():
+                q_home(k, p).start()
+
+        @pl.when(other)
+        def _():
+            kv_z(k, p).start()
+            q_away(k, p).start()
+
+    def take(slot, p):
+        if slot % 4 == 0:
+            @pl.when(other)
+            def _():
+                kv_p(slot, p).wait_recv()
+        else:
+            kv_p(slot, p).wait_recv()
+
+            @pl.when(owner)
+            def _():
+                if slot % 2 == 0:
+                    kv_y(slot, p).start()
+                kv_p(slot, p).start()
+
+    sign = jnp.where(lax.broadcasted_iota(jnp.int32, (1, hw), 1) < hw // 2, -1.0, 1.0)
+
+    def scaled_of(k, p):
+        widened = tok[k, span(p), :].astype(f32)
+        scaled = (widened * gain_ref[...]).astype(bf16)
+        mean = jnp.sum(widened * widened, axis=1, keepdims=True) / width
+        return scaled, lax.rsqrt(mean + NORM_EPS)
+
+    def project_qkv(k, p, scaled, inv_rms):
+        chunk = s if k == 0 else s4
+        near_cos, near_sin = near[0, span(p), :], near[1, span(p), :]
+        far_cos, far_sin = far_ref[chunk, 0:1, :], far_ref[chunk, 1:2, :]
+        cosine = far_cos * near_cos - far_sin * near_sin
+        sine = (far_sin * near_cos + far_cos * near_sin) * sign
+
+        def rotary(v):
+            return v * cosine + pltpu.roll(v, hw // 2, 1) * sine
+
+        out = jnp.dot(scaled, wqkv[...], preferred_element_type=f32) * inv_rms
+        slot = made(k)
+        factor = hw ** (-0.5) * LOG2E
+        queries = [(rotary(out[:, j * hw : (j + 1) * hw]) * factor).astype(bf16) for j in range(2)]
+        for j in range(2):
+            place = slice(pair + j * hw, pair + (j + 1) * hw)
+            kv[slot, span(p), j * hw : (j + 1) * hw] = rotary(out[:, place]).astype(bf16)
+        kv[slot, span(p), pair:] = out[:, 2 * pair :].astype(bf16)
+        stay = owner & (p % 2 == c)
+
+        @pl.when(stay)
+        def _():
+            for j in range(2):
+                q_all[2 * k, q_rows(p), j * hw : (j + 1) * hw] = queries[j]
+
+        @pl.when(jnp.logical_not(stay))
+        def _():
+            for j in range(2):
+                q_stage[k, span(p), j * hw : (j + 1) * hw] = queries[j]
+
+    def own_piece(p):
+        tok_got(0, 2, p)
+        cross_to_p(0, p).start()
+        tok_got(0, 3, p)
+        scaled, inv_rms = scaled_of(0, p)
+        project_qkv(0, p, scaled, inv_rms)
+        inner = jnp.dot(scaled, wconv[0], preferred_element_type=f32) * inv_rms
+        signal = jnp.dot(scaled, wconv[1], preferred_element_type=f32) * inv_rms
+        prod[pl.ds(pl.multiple_of(8 + p * piece, 8), piece), :] = inner * signal
+        gate[span(p), :] = jnp.dot(scaled, wconv[2], preferred_element_type=f32) * inv_rms
+        ship(0, p)
+
+    each(pieces, own_piece)
+
+    edge = remote(prod.at[rows : rows + 8], prod.at[0:8], edge_sem.at[0], edge_sem.at[1], (up, t))
+
+    def far_forward(p):
+        @pl.when(owner)
+        def _():
+            tok_got(1, 0, p)
+            far_to_x(p).start()
+            far_to_p(p).start()
+            tok_got(1, 1, p)
+            mate_back(p).start()
+
+        @pl.when(other)
+        def _():
+            tok_got(1, 0, p)
+            far_to_x(p).start()
+            tok_got(1, 1, p)
+
+    far_forward(0)
+
+    @pl.when(up_ok)
+    def _():
+        edge.start()
+
+    def far_piece(p):
+        @pl.when(p < pieces - 1)
+        def _():
+            far_forward(p + 1)
+
+        tok_got(1, 2, p)
+        cross_to_p(1, p).start()
+        tok_got(1, 3, p)
+        scaled, inv_rms = scaled_of(1, p)
+        project_qkv(1, p, scaled, inv_rms)
+        take(0, p)
+        take(1, p)
+        take(2, p)
+        ship(1, p)
+
+    each(pieces, far_piece)
+
+    @pl.when(down_ok)
+    def _():
+        edge.wait_recv()
+
+    @pl.when(jnp.logical_not(down_ok))
+    def _():
+        prod[0:8, :] = jnp.zeros((8, prod.shape[1]), f32)
+
+    taps = taps_ref[...].astype(f32)
+    for p in range(pieces):
+        begin = 8 + p * piece
+        smoothed = (
+            taps[0:1] * prod[begin - 2 : begin - 2 + piece, :]
+            + taps[1:2] * prod[begin - 1 : begin - 1 + piece, :]
+            + taps[2:3] * prod[begin : begin + piece, :]
+        )
+        convolved = (gate[p * piece : (p + 1) * piece, :] * smoothed).astype(bf16)
+        place = slice((p // 2) * piece, (p // 2 + 1) * piece)
+
+        @pl.when(c == p % 2)
+        def _():
+            cv[c, place, :] = convolved
+
+        @pl.when(c != p % 2)
+        def _():
+            cv_stage[place, :] = convolved
+
+    def more(p):
+        take(3, p)
+        take(6, p)
+        take(4, p)
+        take(5, p)
+
+    each(pieces, more)
+    cv_copy = remote(cv_stage, cv.at[c], cv_send.at[0], cv_recv.at[0], (s, t1))
+    cv_copy.start()
+
+    def xor(a, b):
+        return a + b - 2 * a * b
+
+    def chunk_of(slot):
+        return 4 * xor(zh, slot // 4) + 2 * xor(zl, (slot // 2) % 2) + xor(y, slot % 2)
+
+    def update(jq, m, here, scores, values):
+        old = top[jq, m, here, :]
+        new = jnp.maximum(old, jnp.max(scores, axis=1, keepdims=True))
+        shrink = jnp.exp2(old - new)
+        lifted = jnp.exp2(scores - new[:, :1])
+        top[jq, m, here, :] = new
+        total[jq, m, here, :] = shrink * total[jq, m, here, :] + jnp.sum(lifted, axis=1, keepdims=True)
+        acc[jq, m, here, :] = shrink[:, :1] * acc[jq, m, here, :] + jnp.dot(
+            lifted.astype(bf16), values, preferred_element_type=f32
+        )
+
+    def scores_of(jq, m, here, slot, length):
+        place = slice(m * hw, (m + 1) * hw)
+        return lax.dot_general(
+            q_all[jq, here, place], kv[slot, :length, place], (((1,), (1,)), ((), ())),
+            preferred_element_type=f32,
+        )
+
+    def whole(jq, slot):
+        def sub(i):
+            here = pl.ds(pl.multiple_of(i * piece, 16), piece)
+            for m in range(2):
+                update(jq, m, here, scores_of(jq, m, here, slot, rows), kv[slot, :, pair:])
+
+        each(2, sub)
+
+    def diagonal(jq):
+        slot = 2 * jq
+        for i in range(2):
+            here = slice(i * piece, (i + 1) * piece)
+            length = (2 * i + 2) * piece
+            query_at = (2 * i + c) * piece + lax.broadcasted_iota(jnp.int32, (piece, length), 0)
+            key_at = lax.broadcasted_iota(jnp.int32, (piece, length), 1)
+            for m in range(2):
+                scores = scores_of(jq, m, here, slot, length)
+                scores = jnp.where(key_at <= query_at, scores, MASKED)
+                update(jq, m, here, scores, kv[slot, :length, pair:])
+
+    def q_got(jq):
+        def one(i):
+            here = q_all.at[jq, q_rows(2 * i)]
+            remote(here, here, q_send.at[0, 0], q_recv.at[jq, i], (s, t1)).wait_recv()
+
+        if jq % 2 == 1:
+            each(2, one)
+        else:
+            @pl.when(other)
+            def _():
+                each(2, one)
+
+    q_got(0)
+    q_got(1)
+
+    def near_pair(n):
+        jq, slot = n // 4, n % 4
+
+        @pl.when(chunk_of(slot) < chunk_of(2 * jq))
+        def _():
+            whole(jq, slot)
+
+    each(8, near_pair)
+    each(2, diagonal)
+
+    each(pieces, functools.partial(take, 7))
+    q_got(2)
+    q_got(3)
+
+    def far_pair(n):
+        jq, slot = n // 8, n % 8
+
+        @pl.when((chunk_of(slot) < chunk_of(2 * jq)) & ((jq >= 2) | (slot >= 4)))
+        def _():
+            whole(jq, slot)
+
+    each(32, far_pair)
+    each(4, diagonal, start=2)
+
+    lam_copy.wait_recv()
+    lam = jnp.where(owner, lam_ref[zh, 0:1, 0:1], lam_in[zh, 0:1, 0:1])
+    gain = head_gain_ref[...] * HEAD_KEEP
+    home = 2 * zl + zh
+    seats = (s, s2, s4, s6)
+
+    def att_away(jq, i):
+        part = pl.ds(pl.multiple_of(i * piece, 16), piece)
+        return remote(
+            att_stage.at[jq - 1, part], att.at[home, part], att_send.at[jq - 1, i],
+            att_recv.at[jq - 1, i], (seats[jq], t),
+        )
+
+    def att_got(jq, i):
+        part = pl.ds(pl.multiple_of(i * piece, 16), piece)
+        here = att.at[0, part]
+        remote(here, here, att_send.at[jq - 1, i], att_recv.at[jq - 1, i], (seats[jq], t)).wait_recv()
+
+    def lse_away(jq):
+        return remote(
+            lse_stage.at[jq], lse_in.at[zh, c], lse_send.at[jq], lse_recv.at[zh, c],
+            (seats[jq], 2 * x + zl),
+        )
+
+    for jq in (3, 2, 1, 0):
+        for i in range(2):
+            here = slice(i * piece, (i + 1) * piece)
+            sums = [total[jq, m, here, :] for m in range(2)]
+            parts = [acc[jq, m, here, :] / sums[m][:, :1] for m in range(2)]
+            difference = parts[0] - lam * parts[1]
+            mean = jnp.mean(difference * difference, axis=1, keepdims=True)
+            result = (difference * lax.rsqrt(mean + NORM_EPS) * gain).astype(bf16)
+            if jq == 0:
+                att[home, here, :] = result
+            else:
+                att_stage[jq - 1, here, :] = result
+        tops = [top[jq, m] * (1.0 / LOG2E) + jnp.log(total[jq, m]) for m in range(2)]
+        lane = lax.broadcasted_iota(jnp.int32, tops[0].shape, 1)
+        turned = jnp.where(lane == 0, tops[0], tops[1]).T[0:8, :]
+        if jq == 0:
+            @pl.when(owner)
+            def _():
+                lse_in[zh, c] = turned
+
+            @pl.when(other)
+            def _():
+                lse_stage[jq] = turned
+                lse_away(jq).start()
+        else:
+            lse_stage[jq] = turned
+            for i in range(2):
+                att_away(jq, i).start()
+            lse_away(jq).start()
+
+    for one_copy in wo_copies:
+        one_copy.wait_recv()
+    cv_copy.wait_recv()
+    n_cols = rs_in.shape[0]
+    step = rs_in.shape[2]
+
+    def partial(i, n):
+        part = pl.ds(pl.multiple_of(i * piece, 16), piece)
+        out_cols = pl.ds(pl.multiple_of(n * step, 128), step)
+        result = None
+        for h in range(4):
+            term = jnp.dot(
+                att[h, part, :], wo[h // 2, (h % 2) * pair : (h % 2 + 1) * pair, out_cols],
+                preferred_element_type=f32,
+            )
+            result = term if result is None else result + term
+        for core in range(2):
+            result = result + jnp.dot(cv[core, part, :], wo[2 + core, :, out_cols], preferred_element_type=f32)
+        return result
+
+    def rs_copy(n):
+        return remote(rs_stage.at[n], rs_in.at[n], rs_send.at[n], rs_recv.at[n], (s, t2))
+
+    for jq in (1, 2, 3):
+        att_got(jq, 1 - x)
+
+    def give(n):
+        rs_stage[n] = partial(1 - x, n).astype(bf16)
+        rs_copy(n).start()
+
+    each(n_cols, give)
+    for jq in (1, 2, 3):
+        att_got(jq, x)
+
+    def keep(n):
+        rs_keep[n] = partial(x, n)
+
+    each(n_cols, keep)
+
+    def lse_got(hl, cc):
+        here = lse_in.at[hl, cc]
+
+        @pl.when(jnp.logical_not((zl == c) & (zh == hl) & (cc == c)))
+        def _():
+            remote(here, here, lse_send.at[0], lse_recv.at[hl, cc], (s, t1)).wait_recv()
+
+    for hl in range(2):
+        for cc in range(2):
+            lse_got(hl, cc)
+    lse_ref[...] = lse_in[...]
+
+    for n in range(n_cols):
+        rs_copy(n).wait_recv()
+        out_ref[:, n * step : (n + 1) * step] = (rs_keep[n] + rs_in[n].astype(f32)).astype(bf16)
+
+    lam_copy.wait_send()
+    for one_copy in wo_copies:
+        one_copy.wait_send()
+    cv_copy.wait_send()
+
+    @pl.when(up_ok)
+    def _():
+        edge.wait_send()
+
+    def drain(p):
+        own_to_p(p).wait_send()
+        own_to_x(p).wait_send()
+        far_to_x(p).wait_send()
+        for k in range(2):
+            cross_to_p(k, p).wait_send()
+
+        @pl.when(owner)
+        def _():
+            own_to_f(p).wait_send()
+            mate_to_f(p).wait_send()
+            far_to_p(p).wait_send()
+            mate_back(p).wait_send()
+            for slot in range(8):
+                kv_p(slot, p).wait_send()
+                if slot % 2 == 0:
+                    kv_y(slot, p).wait_send()
+            for k in range(2):
+                @pl.when(p % 2 != c)
+                def _():
+                    q_home(k, p).wait_send()
+
+        @pl.when(other)
+        def _():
+            for k in range(2):
+                kv_z(k, p).wait_send()
+                q_away(k, p).wait_send()
+
+    each(pieces, drain)
+    for jq in (1, 2, 3):
+        for i in range(2):
+            att_away(jq, i).wait_send()
+        lse_away(jq).wait_send()
+
+    @pl.when(other)
+    def _():
+        lse_away(0).wait_send()
+
+    each(n_cols, lambda n: rs_copy(n).wait_send())
+
+
+def whole_layer(
+    tokens, norm_gain, w_query, w_key, w_value, w_outer, w_inner, w_signal, conv_taps, lambdas,
+    head_gain, attend_proj, convolve_proj,
+):
+    rows, block = tokens.shape
+    width = norm_gain.shape[0]
+    chunks = lax.axis_size("sp")
+    head_count = lambdas.shape[0]
+    pair = w_query.shape[1] // head_count
+    channels = w_inner.shape[1]
+    piece = rows // PIECES
+    near, far = table_of(rows, chunks, pair // 2)
+    n_cols = 4
+    step = width // n_cols
+    vmem = pl.BlockSpec(memory_space=pltpu.VMEM)
+    anywhere = pl.BlockSpec(memory_space=pl.ANY)
+    bf16, f32 = jnp.bfloat16, jnp.float32
+    dma = pltpu.SemaphoreType.DMA
+    lam = jnp.broadcast_to(lambdas[:, None, None], (head_count, 8, 128))
+    mixed, lse = pl.pallas_call(
+        layer_kernel,
+        out_shape=(
+            jax.ShapeDtypeStruct((piece, width), bf16),
+            jax.ShapeDtypeStruct((2, 2, 8, 2 * piece), f32),
+        ),
+        in_specs=[anywhere] * 10 + [vmem] * 5,
+        out_specs=(vmem, vmem),
+        scratch_shapes=[
+            pltpu.VMEM((2, rows, width), bf16),
+            pltpu.VMEM((width, 3 * pair), bf16),
+            pltpu.VMEM((3, width, channels), bf16),
+            pltpu.VMEM((4, channels, width), bf16),
+            pltpu.VMEM(near.shape, f32),
+            pltpu.VMEM((10, rows, 2 * pair), bf16),
+            pltpu.VMEM((4, 2 * piece, pair), bf16),
+            pltpu.VMEM((2, rows, pair), bf16),
+            pltpu.VMEM((rows + 8, channels), f32),
+            pltpu.VMEM((rows, channels), f32),
+            pltpu.VMEM((2, 2 * piece, channels), bf16),
+            pltpu.VMEM((2 * piece, channels), bf16),
+            pltpu.VMEM((4, 2 * piece, pair), bf16),
+            pltpu.VMEM((3, 2 * piece, pair), bf16),
+            pltpu.VMEM((2, 2, 8, 2 * piece), f32),
+            pltpu.VMEM((4, 8, 2 * piece), f32),
+            pltpu.VMEM((head_count, 8, 128), f32),
+            pltpu.VMEM((n_cols, piece, step), bf16),
+            pltpu.VMEM((n_cols, piece, step), bf16),
+            pltpu.VMEM((n_cols, piece, step), f32),
+            pltpu.VMEM((4, 2, 2 * piece, pair), f32),
+            pltpu.VMEM((4, 2, 2 * piece, 128), f32),
+            pltpu.VMEM((4, 2, 2 * piece, 128), f32),
+            dma((10,)),
+            dma((9, PIECES)),
+            dma((2, 4, PIECES)),
+            dma((8, PIECES)),
+            dma((4, PIECES)),
+            dma((2, PIECES)),
+            dma((8, PIECES)),
+            dma((2, PIECES)),
+            dma((4, 2)),
+            dma((1,)),
+            dma((1,)),
+            dma((2,)),
+            dma((3, 2)),
+            dma((3, 2)),
+            dma((4,)),
+            dma((2, 2)),
+            dma((2,)),
+            dma((2,)),
+            dma((2,)),
+            dma((n_cols,)),
+            dma((n_cols,)),
+        ],
+        compiler_params=pltpu.CompilerParams(
+            collective_id=0, has_side_effects=True, vmem_limit_bytes=63 * 2**20
+        ),
+        name="whole_layer",
+    )(
+        tokens, w_query, w_key, w_value, w_outer, w_inner, w_signal, jnp.asarray(near), attend_proj,
+        convolve_proj, norm_gain[None, :], jnp.asarray(far), conv_taps, lam, head_gain[None, :],
+    )
+    lse = lse[:, :, :2].reshape(2, 2, 2, 2, piece)
+    lse = jnp.transpose(lse, (3, 1, 4, 0, 2)).reshape(rows, 2 * head_count)
+    return mixed, lse
+
+
 def make_fold(groups, row_count, carry, pieces):
     key_piece, value_piece = pieces
     block_rows = min(key_piece.shape[0], row_count)
@@ -500,6 +1178,12 @@
     head_count = lambdas.shape[0]
     head_width = w_query.shape[1] // (2 * head_count)
     count = lax.axis_size("sp")
+    fits = count == 8 and lax.axis_size("tp") == 4 and head_count == 2 and head_width == 128
+    if fits and row_count % (16 * PIECES) == 0 and w_inner.shape[1] == w_query.shape[1]:
+        return whole_layer(
+            tokens, norm_gain, w_query, w_key, w_value, w_outer, w_inner, w_signal, conv_taps,
+            lambdas, head_gain, attend_proj, convolve_proj,
+        )
     gathered = lax.all_gather(tokens, "tp", axis=1, tiled=True)
     widened = gathered.astype(jnp.float32)
     scaled = (widened * norm_gain[None, :]).astype(jnp.bfloat16)

time: 243 us -> 147 us (0.60)
  waiting for transfers between devices: 136 us -> 0 us
  Pallas kernels: 48.9 us -> 141 us
  matrix products: 22.7 us -> 0 us
  between operations: 14.2 us -> 0.64 us
  other arithmetic: 7.91 us -> 0 us
  starting transfers between devices: 5.55 us -> 0 us
    reduce_scatter x1 -> x0, waiting for transfers between devices: 97.7 us -> none  [per_device(): lax.psum_scatter((jnp.dot(attended, attend_proj, preferred_element_type=j...]
    pallas_call x2 -> x1, Pallas kernels: 48.9 us -> 141 us  [whole_layer(): pl.pallas_call(layer_kernel, out_shape=(jax.ShapeDtypeStruct((piece, widt...]
    all_gather x1 -> x0, waiting for transfers between devices: 28.6 us -> none  [per_device(): gathered = lax.all_gather(tokens, 'tp', axis=1, tiled=True)]
    dot_general x4 -> x0, matrix products: 22.7 us -> none  [the longest x1 10.4 us: per_device(): jnp.dot(convolved, convolve_proj, preferred_element_type=jnp.float32)]
    ppermute x3 -> x0, waiting for transfers between devices: 9.3 us -> none  [the longest x2 9.3 us: partner(): lax.ppermute(value, axis, [(i, i ^ 1 << stride) for i in range(lax.axis_s...]
    ppermute x3 -> x0, starting transfers between devices: 5.48 us -> none  [the longest x1 3.39 us: passed_along(): lax.ppermute(value, axis, [(source, source + steps) for source in range(i...]
    select_n x4 -> x0, other arithmetic: 2.83 us -> none  [the longest x1 1.91 us: attention_by_head(): crossed = partner(jnp.where(at_first, result[1], result[0]), 'sp', 0)]
    reduce_sum x1 -> x0, other arithmetic: 2.72 us -> none  [per_device(): squares = jnp.sum(widened * widened, axis=1)]
  transfers between devices with their start and end apart: 5 -> 0, of which waited for: 3 -> 0; matrix products, arithmetic and copies ran while one was open for 7% -> 0% of each run, Pallas kernels for 20% -> 0%
where the time goes in v1:
time: 147 us
  Pallas kernels  141 us (96%)
  local copies, waits for them, and re-layouts  5.01 us (3%)
    pallas_call x1, Pallas kernels, whole_layer(): pl.pallas_call(layer_kernel, out_shape=(jax.ShapeDtypeStruct((piece, widt...  141 us

profile of v1, /device:TPU:6, one launch (start us, length us, event | category | flops | bytes accessed | tf_op | source)
XLA Modules:
  0.0 146.5 jit_solution(3083916418620789211)
XLA Ops:
  0.6 1.3 broadcast_in_dim.13.lam_ref
  2.0 140.9 %whole_layer.1 = (bf16[192,2048]{1,0:T(8,128)(2,1)}, f32[2,2,8,384]{3,2,1,0:T(8,128)}) custom-call(bf16[768,512]{1,0:T(8,128)(2,1)} %tokens.1, bf16[2048,512]{1,0:T(8,128)(2,1)} %w_query.1, bf16[2048,512]{1,0:T(8,128)(2,1)} %w_key.1, bf16[2048,512]{1,0:T(8,128)(2,1)} %w_value.1, bf16[2048,512]{1,0:T(8,128)(2,1)} %w_outer.1, bf16[2048,512]{1,0:T(8,128)(2,1)} %w_inner.1, ...), custom_call_target="tpu_custom_call" | custom-call | tf_op jit(solution)/shard_map/whole_layer/pallas_call | solution.py:1020
  142.8 0.8 slice.3
  143.6 0.1 reshape.11
  143.7 0.7 reshape.12
  144.4 2.1 %copy.19 = bf16[192,2048]{1,0:T(8,128)(2,1)} copy(bf16[192,2048]{1,0:T(8,128)(2,1)} %get-tuple-element.8) | data formatting | bytes 1572864
  (1 shorter events, 0.0 us)

commit v2 on v1

--- a/solution.py
+++ b/solution.py
@@ -425,7 +425,7 @@
     gain_ref, far_ref, taps_ref, lam_ref, head_gain_ref,
     out_ref, lse_ref,
     tok, wqkv, wconv, wo, near, kv, q_all, q_stage, prod, gate, cv, cv_stage, att, att_stage,
-    lse_in, lse_stage, lam_in, rs_in, rs_stage, rs_keep, acc, top, total,
+    lse_in, lse_stage, lam_stage, lam_in, rs_in, rs_stage, rs_keep, acc, top, total,
     local_sem, tok_send, tok_recv, kv_to_p, kv_to_y, kv_to_z, kv_recv, q_send, q_recv,
     cv_send, cv_recv, edge_sem, att_send, att_recv, lse_send, lse_recv, wo_send, wo_recv,
     lam_sem, rs_send, rs_recv,
@@ -475,6 +475,9 @@
     for load in loads:
         load.start()
 
+    for hl in range(2):
+        lam_stage[hl] = jnp.full(lam_stage.shape[1:], lam_ref[hl], f32)
+
     barrier = pltpu.get_barrier_semaphore()
     peers = [(s1, t), (s2, t), (s4, t), (s6, t), (s, t1), (s, t2), (s2, t1), (s4, t1), (s6, t1)]
     for peer in peers:
@@ -539,16 +542,21 @@
         own_to_p(p).start()
 
     each(pieces, first_sends)
-    lam_copy = remote(lam_ref, lam_in, lam_sem.at[0], lam_sem.at[1], (s, t1))
+    lam_copy = remote(lam_stage, lam_in, lam_sem.at[0], lam_sem.at[1], (s, t1))
     lam_copy.start()
+
+    def to_f(p):
+        @pl.when(owner)
+        def _():
+            own_to_f(p).start()
+            mate_to_f(p).start()
 
     def second_sends(p):
         tok_got(0, 1, p)
 
-        @pl.when(owner)
-        def _():
-            own_to_f(p).start()
-            mate_to_f(p).start()
+        @pl.when(p < 2)
+        def _():
+            to_f(p)
 
     each(pieces, second_sends)
     wo_copies = (
@@ -613,19 +621,18 @@
             kv_z(k, p).start()
             q_away(k, p).start()
 
-    def take(slot, p):
-        if slot % 4 == 0:
-            @pl.when(other)
-            def _():
-                kv_p(slot, p).wait_recv()
-        else:
+    def pass_on(slot, p):
+        @pl.when(owner)
+        def _():
             kv_p(slot, p).wait_recv()
-
-            @pl.when(owner)
-            def _():
-                if slot % 2 == 0:
-                    kv_y(slot, p).start()
-                kv_p(slot, p).start()
+            if slot % 2 == 0:
+                kv_y(slot, p).start()
+            kv_p(slot, p).start()
+
+    def need(slot, low=0, high=PIECES):
+        @pl.when(other)
+        def _():
+            each(high, lambda p: kv_p(slot, p).wait_recv(), start=low)
 
     sign = jnp.where(lax.broadcasted_iota(jnp.int32, (1, hw), 1) < hw // 2, -1.0, 1.0)
 
@@ -665,17 +672,30 @@
             for j in range(2):
                 q_stage[k, span(p), j * hw : (j + 1) * hw] = queries[j]
 
-    def own_piece(p):
-        tok_got(0, 2, p)
-        cross_to_p(0, p).start()
-        tok_got(0, 3, p)
+    def fill(p):
         scaled, inv_rms = scaled_of(0, p)
-        project_qkv(0, p, scaled, inv_rms)
         inner = jnp.dot(scaled, wconv[0], preferred_element_type=f32) * inv_rms
         signal = jnp.dot(scaled, wconv[1], preferred_element_type=f32) * inv_rms
         prod[pl.ds(pl.multiple_of(8 + p * piece, 8), piece), :] = inner * signal
         gate[span(p), :] = jnp.dot(scaled, wconv[2], preferred_element_type=f32) * inv_rms
-        ship(0, p)
+
+    def cross(k, p):
+        tok_got(k, 2, p)
+        cross_to_p(k, p).start()
+
+    def finish_piece(k, p):
+        tok_got(k, 3, p)
+        scaled, inv_rms = scaled_of(k, p)
+        project_qkv(k, p, scaled, inv_rms)
+        ship(k, p)
+
+    def own_piece(p):
+        @pl.when(p == pieces - 1)
+        def _():
+            to_f(2)
+
+        cross(0, p)
+        finish_piece(0, p)
 
     each(pieces, own_piece)
 
@@ -696,28 +716,172 @@
             far_to_x(p).start()
             tok_got(1, 1, p)
 
+    def pass_all(slot, low=0, high=PIECES):
+        each(high, functools.partial(pass_on, slot), start=low)
+
+    def xor(a, b):
+        return a + b - 2 * a * b
+
+    def level_of(k):
+        return 2 * xor(zh, k // 2) + xor(zl, k % 2)
+
+    lanes = top.shape[3]
+
+    def absorb(jq, here, keys, values, seen=None):
+        new_top, lifted, olds = [], [], []
+        for m in range(2):
+            place = slice(m * hw, (m + 1) * hw)
+            scores = lax.dot_general(
+                q_all[jq, here, place], keys(place), (((1,), (1,)), ((), ())),
+                preferred_element_type=f32,
+            )
+            if seen is not None:
+                scores = jnp.where(seen, scores, MASKED)
+            lifted.append(scores)
+            olds.append(top[jq, m, here, :])
+        count = lifted[0].shape[1] // lanes
+        parts = [[v[:, n * lanes : (n + 1) * lanes] for n in range(count)] for v in lifted]
+        for m in range(2):
+            best = functools.reduce(jnp.maximum, parts[m])
+            new_top.append(jnp.maximum(olds[m], jnp.max(best, axis=1, keepdims=True)))
+        raised = [[jnp.exp2(v - new_top[m]) for v in parts[m]] for m in range(2)]
+        shrink = [jnp.exp2(olds[m] - new_top[m]) for m in range(2)]
+        sums = [shrink[m] * total[jq, m, here, :] + functools.reduce(jnp.add, raised[m]) for m in range(2)]
+        block_values = values()
+        added = [
+            jnp.dot(
+                jnp.concatenate([v.astype(bf16) for v in raised[m]], axis=1), block_values,
+                preferred_element_type=f32,
+            )
+            for m in range(2)
+        ]
+        wide = [jnp.concatenate([shrink[m]] * (pair // lanes), axis=1) for m in range(2)]
+        grown = [wide[m] * acc[jq, m, here, :] + added[m] for m in range(2)]
+        for m in range(2):
+            top[jq, m, here, :] = new_top[m]
+            total[jq, m, here, :] = sums[m]
+            acc[jq, m, here, :] = grown[m]
+
+    def part_of(i):
+        return pl.ds(pl.multiple_of(i * piece, 16), piece)
+
+    def both(jq, i, kp, low=0, high=None):
+        high = rows if high is None else high
+
+        def keys(place):
+            return kv[pl.ds(2 * kp, 2), low:high, place].reshape(2 * (high - low), hw)
+
+        def values():
+            return kv[pl.ds(2 * kp, 2), low:high, pair:].reshape(2 * (high - low), pair)
+
+        absorb(jq, part_of(i), keys, values)
+
+    def beside(jq, i):
+        slot = 2 * jq + 1
+        absorb(jq, part_of(i), lambda place: kv[slot, :, place], lambda: kv[slot, :, pair:])
+
+    def diagonal(jq, i):
+        slot = 2 * jq
+        for half in range(2):
+            @pl.when(i == half)
+            def _():
+                length = (2 * half + 2) * piece
+                query_at = (2 * half + c) * piece + lax.broadcasted_iota(jnp.int32, (piece, length), 0)
+                key_at = lax.broadcasted_iota(jnp.int32, (piece, length), 1)
+                absorb(
+                    jq, part_of(i), lambda place: kv[slot, :length, place],
+                    lambda: kv[slot, :length, pair:], key_at <= query_at,
+                )
+
+    def q_got(jq, i):
+        def one():
+            here = q_all.at[jq, q_rows(2 * i)]
+            remote(here, here, q_send.at[0, 0], q_recv.at[jq, i], (s, t1)).wait_recv()
+
+        if jq % 2 == 1:
+            one()
+        else:
+            pl.when(other)(one)
+
     far_forward(0)
+    to_f(3)
+    far_forward(1)
+    fill(0)
+    pass_all(1)
+    cross(1, 0)
+
+    def far_piece(p):
+        finish_piece(1, p)
+
+        @pl.when((p > 0) & (p < pieces - 1))
+        def _():
+            far_forward(p + 1)
+
+        @pl.when(p == 1)
+        def _():
+            pass_all(2)
+
+        @pl.when(p < pieces - 1)
+        def _():
+            fill(p + 1)
+
+            @pl.when(p == 1)
+            def _():
+                need(0)
+                q_got(0, 0)
+                q_got(0, 1)
+                each(2, lambda i: diagonal(0, i))
+
+            cross(1, p + 1)
+
+    each(pieces, far_piece)
 
     @pl.when(up_ok)
     def _():
         edge.start()
 
-    def far_piece(p):
-        @pl.when(p < pieces - 1)
-        def _():
-            far_forward(p + 1)
-
-        tok_got(1, 2, p)
-        cross_to_p(1, p).start()
-        tok_got(1, 3, p)
-        scaled, inv_rms = scaled_of(1, p)
-        project_qkv(1, p, scaled, inv_rms)
-        take(0, p)
-        take(1, p)
-        take(2, p)
-        ship(1, p)
-
-    each(pieces, far_piece)
+    half = pieces // 2
+    pass_on(6, 0)
+    pass_all(5, 0, 3)
+    need(2)
+    q_got(1, 0)
+    q_got(1, 1)
+    each(2, lambda i: diagonal(1, i))
+    pass_on(6, 1)
+    pass_all(3)
+
+    def near_level(n):
+        jq, i = n // 2, n % 2
+
+        @pl.when(level_of(1 - jq) < level_of(jq))
+        def _():
+            both(jq, i, 1 - jq)
+
+        @pl.when(y == 1)
+        def _():
+            beside(jq, i)
+
+    need(1)
+    need(3)
+    each(4, near_level)
+    pass_on(6, 2)
+    pass_on(5, 3)
+    pass_all(7, 0, half)
+    for slot in (4, 5, 6, 7):
+        need(slot, 0, half)
+    q_got(2, 0)
+    q_got(3, 0)
+
+    @pl.when(zh == 1)
+    def _():
+        each(8, lambda n: both(n // 4, (n // 2) % 2, 2 + n % 2, 0, halves))
+
+    @pl.when(zh == 0)
+    def _():
+        each(4, lambda n: both(2 + n // 2, 0, n % 2))
+
+    pass_on(6, 3)
+    pass_on(7, 2)
 
     @pl.when(down_ok)
     def _():
@@ -746,156 +910,94 @@
         def _():
             cv_stage[place, :] = convolved
 
-    def more(p):
-        take(3, p)
-        take(6, p)
-        take(4, p)
-        take(5, p)
-
-    each(pieces, more)
     cv_copy = remote(cv_stage, cv.at[c], cv_send.at[0], cv_recv.at[0], (s, t1))
     cv_copy.start()
 
-    def xor(a, b):
-        return a + b - 2 * a * b
-
-    def chunk_of(slot):
-        return 4 * xor(zh, slot // 4) + 2 * xor(zl, (slot // 2) % 2) + xor(y, slot % 2)
-
-    def update(jq, m, here, scores, values):
-        old = top[jq, m, here, :]
-        new = jnp.maximum(old, jnp.max(scores, axis=1, keepdims=True))
-        shrink = jnp.exp2(old - new)
-        lifted = jnp.exp2(scores - new[:, :1])
-        top[jq, m, here, :] = new
-        total[jq, m, here, :] = shrink * total[jq, m, here, :] + jnp.sum(lifted, axis=1, keepdims=True)
-        acc[jq, m, here, :] = shrink[:, :1] * acc[jq, m, here, :] + jnp.dot(
-            lifted.astype(bf16), values, preferred_element_type=f32
-        )
-
-    def scores_of(jq, m, here, slot, length):
-        place = slice(m * hw, (m + 1) * hw)
-        return lax.dot_general(
-            q_all[jq, here, place], kv[slot, :length, place], (((1,), (1,)), ((), ())),
-            preferred_element_type=f32,
-        )
-
-    def whole(jq, slot):
-        def sub(i):
-            here = pl.ds(pl.multiple_of(i * piece, 16), piece)
-            for m in range(2):
-                update(jq, m, here, scores_of(jq, m, here, slot, rows), kv[slot, :, pair:])
-
-        each(2, sub)
-
-    def diagonal(jq):
-        slot = 2 * jq
-        for i in range(2):
-            here = slice(i * piece, (i + 1) * piece)
-            length = (2 * i + 2) * piece
-            query_at = (2 * i + c) * piece + lax.broadcasted_iota(jnp.int32, (piece, length), 0)
-            key_at = lax.broadcasted_iota(jnp.int32, (piece, length), 1)
-            for m in range(2):
-                scores = scores_of(jq, m, here, slot, length)
-                scores = jnp.where(key_at <= query_at, scores, MASKED)
-                update(jq, m, here, scores, kv[slot, :length, pair:])
-
-    def q_got(jq):
-        def one(i):
-            here = q_all.at[jq, q_rows(2 * i)]
-            remote(here, here, q_send.at[0, 0], q_recv.at[jq, i], (s, t1)).wait_recv()
-
-        if jq % 2 == 1:
-            each(2, one)
-        else:
-            @pl.when(other)
-            def _():
-                each(2, one)
-
-    q_got(0)
-    q_got(1)
-
-    def near_pair(n):
-        jq, slot = n // 4, n % 4
-
-        @pl.when(chunk_of(slot) < chunk_of(2 * jq))
-        def _():
-            whole(jq, slot)
-
-    each(8, near_pair)
-    each(2, diagonal)
-
-    each(pieces, functools.partial(take, 7))
-    q_got(2)
-    q_got(3)
-
-    def far_pair(n):
-        jq, slot = n // 8, n % 8
-
-        @pl.when((chunk_of(slot) < chunk_of(2 * jq)) & ((jq >= 2) | (slot >= 4)))
-        def _():
-            whole(jq, slot)
-
-    each(32, far_pair)
-    each(4, diagonal, start=2)
+    pass_on(7, 3)
+    for slot in (4, 5, 6, 7):
+        need(slot, half)
+    q_got(2, 1)
+    q_got(3, 1)
 
     lam_copy.wait_recv()
-    lam = jnp.where(owner, lam_ref[zh, 0:1, 0:1], lam_in[zh, 0:1, 0:1])
+    lam = jnp.where(owner, lam_stage[zh, 0:1, :], lam_in[zh, 0:1, :])
+    lam = jnp.concatenate([lam] * (pair // lanes), axis=1)
     gain = head_gain_ref[...] * HEAD_KEEP
     home = 2 * zl + zh
-    seats = (s, s2, s4, s6)
+
+    def seat(jq):
+        return 2 * level_of(jq) + y
 
     def att_away(jq, i):
-        part = pl.ds(pl.multiple_of(i * piece, 16), piece)
         return remote(
-            att_stage.at[jq - 1, part], att.at[home, part], att_send.at[jq - 1, i],
-            att_recv.at[jq - 1, i], (seats[jq], t),
+            att_stage.at[jq - 1, part_of(i)], att.at[home, part_of(i)], att_send.at[jq - 1, i],
+            att_recv.at[jq - 1, i], (seat(jq), t),
         )
 
     def att_got(jq, i):
-        part = pl.ds(pl.multiple_of(i * piece, 16), piece)
-        here = att.at[0, part]
-        remote(here, here, att_send.at[jq - 1, i], att_recv.at[jq - 1, i], (seats[jq], t)).wait_recv()
+        here = att.at[0, part_of(i)]
+        remote(here, here, att_send.at[jq - 1, i], att_recv.at[jq - 1, i], (seat(jq), t)).wait_recv()
 
     def lse_away(jq):
         return remote(
             lse_stage.at[jq], lse_in.at[zh, c], lse_send.at[jq], lse_recv.at[zh, c],
-            (seats[jq], 2 * x + zl),
-        )
-
-    for jq in (3, 2, 1, 0):
-        for i in range(2):
-            here = slice(i * piece, (i + 1) * piece)
-            sums = [total[jq, m, here, :] for m in range(2)]
-            parts = [acc[jq, m, here, :] / sums[m][:, :1] for m in range(2)]
-            difference = parts[0] - lam * parts[1]
-            mean = jnp.mean(difference * difference, axis=1, keepdims=True)
-            result = (difference * lax.rsqrt(mean + NORM_EPS) * gain).astype(bf16)
-            if jq == 0:
-                att[home, here, :] = result
-            else:
-                att_stage[jq - 1, here, :] = result
-        tops = [top[jq, m] * (1.0 / LOG2E) + jnp.log(total[jq, m]) for m in range(2)]
-        lane = lax.broadcasted_iota(jnp.int32, tops[0].shape, 1)
-        turned = jnp.where(lane == 0, tops[0], tops[1]).T[0:8, :]
-        if jq == 0:
-            @pl.when(owner)
+            (seat(jq), 2 * x + zl),
+        )
+
+    def close(jq, i):
+        here = part_of(i)
+        parts = [
+            acc[jq, m, here, :] / jnp.sum(total[jq, m, here, :], axis=1, keepdims=True) for m in range(2)
+        ]
+        difference = parts[0] - lam * parts[1]
+        mean = jnp.mean(difference * difference, axis=1, keepdims=True)
+        result = (difference * lax.rsqrt(mean + NORM_EPS) * gain).astype(bf16)
+
+        @pl.when(jq == 0)
+        def _():
+            att[home, here, :] = result
+
+        @pl.when(jq > 0)
+        def _():
+            att_stage[jq - 1, here, :] = result
+            att_away(jq, i).start()
+
+    def one_slot(i, n):
+        jq = jnp.where(n < 2, n + 2, 3 - n)
+
+        def one_level(kp):
+            @pl.when((level_of(kp) < level_of(jq)) & (jq >= 2) & ((kp >= 2) | (i == 1)))
             def _():
-                lse_in[zh, c] = turned
-
-            @pl.when(other)
+                both(jq, i, kp)
+
+            @pl.when((level_of(kp) < level_of(jq)) & (jq < 2) & (kp >= 2))
             def _():
-                lse_stage[jq] = turned
-                lse_away(jq).start()
-        else:
-            lse_stage[jq] = turned
-            for i in range(2):
-                att_away(jq, i).start()
-            lse_away(jq).start()
-
-    for one_copy in wo_copies:
-        one_copy.wait_recv()
-    cv_copy.wait_recv()
+                both(jq, i, kp, halves, rows)
+
+        each(4, one_level)
+
+        @pl.when(jq >= 2)
+        def _():
+            @pl.when(y == 1)
+            def _():
+                beside(jq, i)
+
+            diagonal(jq, i)
+
+        close(jq, i)
+
+    def one_job(n):
+        @pl.when(n == 6)
+        def _():
+            cv_copy.wait_recv()
+            for one_copy in wo_copies:
+                one_copy.wait_recv()
+            for jq in (1, 2, 3):
+                att_got(jq, 1 - x)
+            each(n_cols, give)
+
+        one_slot(jnp.where(n < 4, 1 - x, x), n % 4)
+
     n_cols = rs_in.shape[0]
     step = rs_in.shape[2]
 
@@ -916,14 +1018,11 @@
     def rs_copy(n):
         return remote(rs_stage.at[n], rs_in.at[n], rs_send.at[n], rs_recv.at[n], (s, t2))
 
-    for jq in (1, 2, 3):
-        att_got(jq, 1 - x)
-
     def give(n):
         rs_stage[n] = partial(1 - x, n).astype(bf16)
         rs_copy(n).start()
 
-    each(n_cols, give)
+    each(8, one_job)
     for jq in (1, 2, 3):
         att_got(jq, x)
 
@@ -931,6 +1030,26 @@
         rs_keep[n] = partial(x, n)
 
     each(n_cols, keep)
+
+    for jq in (3, 2, 1, 0):
+        tops = [
+            top[jq, m] * (1.0 / LOG2E) + jnp.log(jnp.sum(total[jq, m], axis=1, keepdims=True))
+            for m in range(2)
+        ]
+        lane = lax.broadcasted_iota(jnp.int32, tops[0].shape, 1)
+        turned = jnp.where(lane == 0, tops[0], tops[1]).T[0:8, :]
+        if jq == 0:
+            @pl.when(owner)
+            def _():
+                lse_in[zh, c] = turned
+
+            @pl.when(other)
+            def _():
+                lse_stage[jq] = turned
+                lse_away(jq).start()
+        else:
+            lse_stage[jq] = turned
+            lse_away(jq).start()
 
     def lse_got(hl, cc):
         here = lse_in.at[hl, cc]
@@ -942,7 +1061,13 @@
     for hl in range(2):
         for cc in range(2):
             lse_got(hl, cc)
-    lse_ref[...] = lse_in[...]
+    for cc in range(2):
+        both_heads = jnp.concatenate(
+            [lse_in[0, cc, 0:2], lse_in[1, cc, 0:2], jnp.zeros((lanes - 4, halves), f32)], axis=0
+        ).T
+        for i in range(2):
+            begin = (2 * i + cc) * piece
+            lse_ref[begin : begin + piece, :] = both_heads[i * piece : (i + 1) * piece, 0:4]
 
     for n in range(n_cols):
         rs_copy(n).wait_recv()
@@ -1016,14 +1141,13 @@
     anywhere = pl.BlockSpec(memory_space=pl.ANY)
     bf16, f32 = jnp.bfloat16, jnp.float32
     dma = pltpu.SemaphoreType.DMA
-    lam = jnp.broadcast_to(lambdas[:, None, None], (head_count, 8, 128))
     mixed, lse = pl.pallas_call(
         layer_kernel,
         out_shape=(
             jax.ShapeDtypeStruct((piece, width), bf16),
-            jax.ShapeDtypeStruct((2, 2, 8, 2 * piece), f32),
+            jax.ShapeDtypeStruct((rows, 2 * head_count), f32),
         ),
-        in_specs=[anywhere] * 10 + [vmem] * 5,
+        in_specs=[anywhere] * 10 + [vmem] * 3 + [pl.BlockSpec(memory_space=pltpu.SMEM), vmem],
         out_specs=(vmem, vmem),
         scratch_shapes=[
             pltpu.VMEM((2, rows, width), bf16),
@@ -1042,6 +1166,7 @@
             pltpu.VMEM((3, 2 * piece, pair), bf16),
             pltpu.VMEM((2, 2, 8, 2 * piece), f32),
             pltpu.VMEM((4, 8, 2 * piece), f32),
+            pltpu.VMEM((head_count, 8, 128), f32),
             pltpu.VMEM((head_count, 8, 128), f32),
             pltpu.VMEM((n_cols, piece, step), bf16),
             pltpu.VMEM((n_cols, piece, step), bf16),
@@ -1077,10 +1202,8 @@
         name="whole_layer",
     )(
         tokens, w_query, w_key, w_value, w_outer, w_inner, w_signal, jnp.asarray(near), attend_proj,
-        convolve_proj, norm_gain[None, :], jnp.asarray(far), conv_taps, lam, head_gain[None, :],
-    )
-    lse = lse[:, :, :2].reshape(2, 2, 2, 2, piece)
-    lse = jnp.transpose(lse, (3, 1, 4, 0, 2)).reshape(rows, 2 * head_count)
+        convolve_proj, norm_gain[None, :], jnp.asarray(far), conv_taps, lambdas, head_gain[None, :],
+    )
     return mixed, lse
 
 

time: 147 us -> 116 us (0.79)
  Pallas kernels: 141 us -> 110 us
    pallas_call x1, Pallas kernels: 141 us -> 110 us  [whole_layer(): pl.pallas_call(layer_kernel, out_shape=(jax.ShapeDtypeStruct((piece, widt...]
    pallas_call x0 -> x1, local copies, waits for them, and re-layouts: none -> 1.75 us  [whole_layer(): pl.pallas_call(layer_kernel, out_shape=(jax.ShapeDtypeStruct((piece, widt...]
where the time goes in v2:
time: 116 us; the launch traced here: 115 us
  Pallas kernels  110 us (95%)
  local copies, waits for them, and re-layouts  3.83 us (3%)
    pallas_call x1, Pallas kernels, whole_layer(): pl.pallas_call(layer_kernel, out_shape=(jax.ShapeDtypeStruct((piece, widt...  110 us

profile of v2, /device:TPU:6, one launch (start us, length us, event | category | flops | bytes accessed | tf_op | source)
XLA Modules:
  0.0 114.7 jit_solution(10799906567991631580)
XLA Ops:
  0.6 110.2 %whole_layer.1 = (bf16[192,2048]{1,0:T(8,128)(2,1)}, f32[768,4]{1,0:T(8,128)}) custom-call(bf16[768,512]{1,0:T(8,128)(2,1)} %tokens.1, bf16[2048,512]{1,0:T(8,128)(2,1)} %w_query.1, bf16[2048,512]{1,0:T(8,128)(2,1)} %w_key.1, bf16[2048,512]{1,0:T(8,128)(2,1)} %w_value.1, bf16[2048,512]{1,0:T(8,128)(2,1)} %w_outer.1, bf16[2048,512]{1,0:T(8,128)(2,1)} %w_inner.1, ...), custom_call_target="tpu_custom_call" | custom-call | tf_op jit(solution)/shard_map/whole_layer/pallas_call | solution.py:1144
  110.8 1.7 %copy.17 = f32[768,4]{0,1:T(4,128)} copy(f32[768,4]{1,0:T(8,128)} %get-tuple-element.3) | data formatting | bytes 24576 | tf_op jit(solution)/shard_map/whole_layer/pallas_call | solution.py:1144
  112.6 2.1 %copy.19 = bf16[192,2048]{1,0:T(8,128)(2,1)} copy(bf16[192,2048]{1,0:T(8,128)(2,1)} %get-tuple-element.6) | data formatting | bytes 1572864

commit v3 on v2

--- a/solution.py
+++ b/solution.py
@@ -821,6 +821,10 @@
         def _():
             pass_all(2)
 
+        @pl.when(p == 3)
+        def _():
+            pass_on(6, 0)
+
         @pl.when(p < pieces - 1)
         def _():
             fill(p + 1)
@@ -840,8 +844,53 @@
     def _():
         edge.start()
 
+    lam_copy.wait_recv()
+    lam = jnp.where(owner, lam_stage[zh, 0:1, :], lam_in[zh, 0:1, :])
+    lam = jnp.concatenate([lam] * (pair // lanes), axis=1)
+    gain = head_gain_ref[...] * HEAD_KEEP
+    home = 2 * zl + zh
+
+    def seat(jq):
+        return 2 * level_of(jq) + y
+
+    def att_away(jq, i):
+        return remote(
+            att_stage.at[jq - 1, part_of(i)], att.at[home, part_of(i)], att_send.at[jq - 1, i],
+            att_recv.at[jq - 1, i], (seat(jq), t),
+        )
+
+    def att_got(jq, i):
+        here = att.at[0, part_of(i)]
+        remote(here, here, att_send.at[jq - 1, i], att_recv.at[jq - 1, i], (seat(jq), t)).wait_recv()
+
+    def lse_away(jq):
+        return remote(
+            lse_stage.at[jq], lse_in.at[zh, c], lse_send.at[jq], lse_recv.at[zh, c],
+            (seat(jq), 2 * x + zl),
+        )
+
+    def close(jq, i, now):
+        here = part_of(i)
+        parts = [
+            acc[jq, m, here, :] / jnp.sum(total[jq, m, here, :], axis=1, keepdims=True) for m in range(2)
+        ]
+        difference = parts[0] - lam * parts[1]
+        mean = jnp.mean(difference * difference, axis=1, keepdims=True)
+        result = (difference * lax.rsqrt(mean + NORM_EPS) * gain).astype(bf16)
+
+        @pl.when(jq == 0)
+        def _():
+            att[home, here, :] = result
+
+        @pl.when(jq > 0)
+        def _():
+            att_stage[jq - 1, here, :] = result
+
+            @pl.when(now)
+            def _():
+                att_away(jq, i).start()
+
     half = pieces // 2
-    pass_on(6, 0)
     pass_all(5, 0, 3)
     need(2)
     q_got(1, 0)
@@ -864,6 +913,11 @@
     need(1)
     need(3)
     each(4, near_level)
+
+    @pl.when(zh == 0)
+    def _():
+        each(4, lambda n: close(1 - n // 2, n % 2, True))
+
     pass_on(6, 2)
     pass_on(5, 3)
     pass_all(7, 0, half)
@@ -882,6 +936,12 @@
 
     pass_on(6, 3)
     pass_on(7, 2)
+    q_got(2, 1)
+    q_got(3, 1)
+
+    @pl.when(zh == 0)
+    def _():
+        each(4, lambda n: both(2 + n // 2, 1, n % 2))
 
     @pl.when(down_ok)
     def _():
@@ -916,57 +976,12 @@
     pass_on(7, 3)
     for slot in (4, 5, 6, 7):
         need(slot, half)
-    q_got(2, 1)
-    q_got(3, 1)
-
-    lam_copy.wait_recv()
-    lam = jnp.where(owner, lam_stage[zh, 0:1, :], lam_in[zh, 0:1, :])
-    lam = jnp.concatenate([lam] * (pair // lanes), axis=1)
-    gain = head_gain_ref[...] * HEAD_KEEP
-    home = 2 * zl + zh
-
-    def seat(jq):
-        return 2 * level_of(jq) + y
-
-    def att_away(jq, i):
-        return remote(
-            att_stage.at[jq - 1, part_of(i)], att.at[home, part_of(i)], att_send.at[jq - 1, i],
-            att_recv.at[jq - 1, i], (seat(jq), t),
-        )
-
-    def att_got(jq, i):
-        here = att.at[0, part_of(i)]
-        remote(here, here, att_send.at[jq - 1, i], att_recv.at[jq - 1, i], (seat(jq), t)).wait_recv()
-
-    def lse_away(jq):
-        return remote(
-            lse_stage.at[jq], lse_in.at[zh, c], lse_send.at[jq], lse_recv.at[zh, c],
-            (seat(jq), 2 * x + zl),
-        )
-
-    def close(jq, i):
-        here = part_of(i)
-        parts = [
-            acc[jq, m, here, :] / jnp.sum(total[jq, m, here, :], axis=1, keepdims=True) for m in range(2)
-        ]
-        difference = parts[0] - lam * parts[1]
-        mean = jnp.mean(difference * difference, axis=1, keepdims=True)
-        result = (difference * lax.rsqrt(mean + NORM_EPS) * gain).astype(bf16)
-
-        @pl.when(jq == 0)
-        def _():
-            att[home, here, :] = result
-
-        @pl.when(jq > 0)
-        def _():
-            att_stage[jq - 1, here, :] = result
-            att_away(jq, i).start()
-
-    def one_slot(i, n):
+
+    def one_slot(i, n, now):
         jq = jnp.where(n < 2, n + 2, 3 - n)
 
         def one_level(kp):
-            @pl.when((level_of(kp) < level_of(jq)) & (jq >= 2) & ((kp >= 2) | (i == 1)))
+            @pl.when((level_of(kp) < level_of(jq)) & (jq >= 2) & (kp >= 2))
             def _():
                 both(jq, i, kp)
 
@@ -984,7 +999,9 @@
 
             diagonal(jq, i)
 
-        close(jq, i)
+        @pl.when((jq >= 2) | (zh == 1))
+        def _():
+            close(jq, i, now)
 
     def one_job(n):
         @pl.when(n == 6)
@@ -995,8 +1012,10 @@
             for jq in (1, 2, 3):
                 att_got(jq, 1 - x)
             each(n_cols, give)
-
-        one_slot(jnp.where(n < 4, 1 - x, x), n % 4)
+            for jq in (2, 3):
+                att_away(jq, x).start()
+
+        one_slot(jnp.where(n < 4, 1 - x, x), n % 4, (n < 4) | (n >= 6))
 
     n_cols = rs_in.shape[0]
     step = rs_in.shape[2]
@@ -1023,14 +1042,6 @@
         rs_copy(n).start()
 
     each(8, one_job)
-    for jq in (1, 2, 3):
-        att_got(jq, x)
-
-    def keep(n):
-        rs_keep[n] = partial(x, n)
-
-    each(n_cols, keep)
-
     for jq in (3, 2, 1, 0):
         tops = [
             top[jq, m] * (1.0 / LOG2E) + jnp.log(jnp.sum(total[jq, m], axis=1, keepdims=True))
@@ -1050,6 +1061,14 @@
         else:
             lse_stage[jq] = turned
             lse_away(jq).start()
+
+    for jq in (1, 2, 3):
+        att_got(jq, x)
+
+    def keep(n):
+        rs_keep[n] = partial(x, n)
+
+    each(n_cols, keep)
 
     def lse_got(hl, cc):
         here = lse_in.at[hl, cc]

time: 116 us -> 113 us (0.974)
  Pallas kernels: 110 us -> 106 us
    pallas_call x1, Pallas kernels: 110 us -> 106 us  [whole_layer(): pl.pallas_call(layer_kernel, out_shape=(jax.ShapeDtypeStruct((piece, widt...]
where the time goes in v3:
time: 113 us; the launch traced here: 111 us
  Pallas kernels  106 us (94%)
  local copies, waits for them, and re-layouts  3.83 us (3%)
    pallas_call x1, Pallas kernels, whole_layer(): pl.pallas_call(layer_kernel, out_shape=(jax.ShapeDtypeStruct((piece, widt...  106 us

profile of v3, /device:TPU:6, one launch (start us, length us, event | category | flops | bytes accessed | tf_op | source)
XLA Modules:
  0.0 111.0 jit_solution(4536044116981148977)
XLA Ops:
  0.6 106.5 %whole_layer.1 = (bf16[192,2048]{1,0:T(8,128)(2,1)}, f32[768,4]{1,0:T(8,128)}) custom-call(bf16[768,512]{1,0:T(8,128)(2,1)} %tokens.1, bf16[2048,512]{1,0:T(8,128)(2,1)} %w_query.1, bf16[2048,512]{1,0:T(8,128)(2,1)} %w_key.1, bf16[2048,512]{1,0:T(8,128)(2,1)} %w_value.1, bf16[2048,512]{1,0:T(8,128)(2,1)} %w_outer.1, bf16[2048,512]{1,0:T(8,128)(2,1)} %w_inner.1, ...), custom_call_target="tpu_custom_call" | custom-call | tf_op jit(solution)/shard_map/whole_layer/pallas_call | solution.py:1163
  107.1 1.7 %copy.17 = f32[768,4]{0,1:T(4,128)} copy(f32[768,4]{1,0:T(8,128)} %get-tuple-element.3) | data formatting | bytes 24576 | tf_op jit(solution)/shard_map/whole_layer/pallas_call | solution.py:1163
  108.9 2.1 %copy.19 = bf16[192,2048]{1,0:T(8,128)(2,1)} copy(bf16[192,2048]{1,0:T(8,128)(2,1)} %get-tuple-element.6) | data formatting | bytes 1572864
